TPU v7x, 512 devices: a whole 4x4x16 slice. The times are simulated.
512 devices in a mesh: sp: 64 (over z, y), tp: 8 (over x, core).
Axes of the slice: x: 4, y: 4, z: 16, core: 2. Of those that a mesh axis runs over, the one named last changes fastest.
Arguments:
- queries: bfloat16 [24576, 2048], P('sp', 'tp'), may hold values from -6 to 6
- key_heads: bfloat16 [24576, 1024], P('sp', 'tp'), may hold values from -6 to 6
- value_heads: bfloat16 [24576, 1024], P('sp', 'tp'), may hold values from -6 to 6
- sink_logit: float32 [16], P('tp'), may hold values from 3 to 7
- doc_ids: int32 [24576], replicated, may hold values from 0 to 15, never falling along the last dimension, each value on 1 to 3072 neighbouring positions
- residual: bfloat16 [24576, 2048], P('sp'), may hold values from -6 to 6
- out_proj: bfloat16 [2048, 2048], P('tp'), may hold values from -0.125 to 0.125
- gain_mix: float32 [2048], replicated, may hold values from 0.1 to 1.9
- up_proj: bfloat16 [2048, 8192], P('sp', 'tp'), may hold values from -0.125 to 0.125
- down_proj: bfloat16 [8192, 2048], P('tp', 'sp'), may hold values from -0.0625 to 0.0625
- gain_ffn_in: float32 [2048], replicated, may hold values from 0.1 to 1.9
- gain_ffn_out: float32 [2048], replicated, may hold values from 0.1 to 1.9
Outputs:
- layer_out: bfloat16 [24576, 2048], P(('sp', 'tp'))
All inputs are finite; a program needn't handle non-finite values.
Results may differ from a plain program's by a relative error of at most 0.019.
Values may be sent and summed in bfloat16 or wider, within the bound.
No kernel may reach another device: no remote copies, remote signals or barrier semaphores. Data moves between devices by JAX's collectives and lax.ppermute only.
A program may use at most 64 MiB of HBM per device.

v0:
```python
import jax
import jax.numpy as jnp
from jax import lax
from jax.sharding import PartitionSpec as P

HD = 128
WINDOW = 128


def fetch(shard, ahead, aside):
    pairs = [
        (4 * ((z + ahead) % 16) + (y + aside) % 4, 4 * z + y) for z in range(16) for y in range(4)
    ]
    return lax.ppermute(shard, "sp", pairs)


def placed(own, pieces, dim, own_at):
    whole = jnp.expand_dims(own, dim)
    whole = jnp.broadcast_to(whole, (*whole.shape[:dim], 4, *whole.shape[dim + 1 :]))
    for piece, away, cut, start in pieces:
        at = [0] * whole.ndim
        at[cut] = start
        at[dim] = (own_at + away) % 4
        whole = lax.dynamic_update_slice(whole, jnp.expand_dims(piece, dim), at)
    return whole


def far_stage(shard):
    rows = [(z % 4, y, 4 * z + y) for z in range(16) for y in range(4)]
    groups = [[i for a, b, i in rows if (a, b) == (c, d)] for c in range(4) for d in range(4)]
    spread = jnp.broadcast_to(shard[None], (4, *shard.shape))
    return lax.all_to_all(spread, "sp", 0, 0, axis_index_groups=groups, tiled=True)


def beside(shard, along):
    if along == "z":
        return fetch(shard, 1, 0), fetch(shard, -1, 0)
    return fetch(shard, 0, 1), fetch(shard, 0, -1)


def across_z(shard):
    half = shard.shape[0] // 2
    return fetch(shard[:half], 2, 0), fetch(shard[half:], -2, 0)


def joined_z(shard, near, far, dim, own_at):
    half = shard.shape[0] // 2
    pieces = [(near[0], 1, 0, 0), (near[1], 3, 0, 0)]
    pieces += [(far[0], 2, 0, 0), (far[1], 2, 0, half)]
    return placed(shard, pieces, dim, own_at)


def joined_y(shard, near, far, dim, own_at):
    pieces = [(near[0], 1, 0, 0), (near[1], 3, 0, 0), (far, 2, 0, 0)]
    return placed(shard, pieces, dim, own_at)


def start_weights(up_proj, down_proj):
    place = lax.axis_index("sp")
    z, y = (place // 4, place % 4)
    far = far_stage(jnp.stack([up_proj, down_proj.T]))
    up, down = (far[:, 0], far[:, 1])
    up = joined_y(up, beside(up, "y"), fetch(up, 0, 2), 1, y)
    down = joined_z(down, beside(down, "z"), across_z(down), 1, z % 4)
    return up, down, beside(up, "z"), beside(down, "y")


def finish_weights(up, down, up_near, down_near):
    place = lax.axis_index("sp")
    z, y = (place // 4, place % 4)
    up_far, down_far = (across_z(up), fetch(down, 0, 2))
    up_whole = joined_z(up, up_near, up_far, 1, z % 4)
    down_whole = joined_y(down, down_near, down_far, 2, y)
    return up_whole.reshape(2048, -1), down_whole.reshape(2048, -1)


def padded(shard, sides, width):
    for axis, dim in sides:
        devices, length = (lax.axis_size(axis), shard.shape[dim])
        up = [(i, (i + 1) % devices) for i in range(devices - 1)]
        down = [(j, i) for i, j in up]
        last = lax.slice_in_dim(shard, length - width, length, axis=dim)
        first = lax.slice_in_dim(shard, 0, width, axis=dim)
        before = lax.ppermute(last, axis, up)
        after = lax.ppermute(first, axis, down)
        shard = jnp.concatenate([before, shard, after], axis=dim)
    return shard


def split_up(shard, dim, devices):
    before, after = (shard.shape[:dim], shard.shape[dim + 1 :])
    return jnp.moveaxis(shard.reshape(*before, devices, -1, *after), dim, 0)


def summed_on_arrival(shard, axis, dim):
    pieces = split_up(shard, dim, lax.axis_size(axis))
    arrived = lax.all_to_all(pieces, axis, split_axis=0, concat_axis=0, tiled=True)
    return arrived.astype(jnp.float32).sum(axis=0)


def joined_along(pieces, dim):
    pieces = jnp.moveaxis(pieces, 0, dim)
    lengths = pieces.shape
    return pieces.reshape(*lengths[:dim], lengths[dim] * lengths[dim + 1], *lengths[dim + 2 :])


def copy_for_each(shard, axis):
    devices = lax.axis_size(axis)
    return lax.all_to_all(
        jnp.broadcast_to(shard[None], (devices, *shard.shape)), axis, 0, 0, tiled=True
    )


def collect(shard, axis, dim):
    return joined_along(copy_for_each(shard, axis), dim)


def rotate(field, places):
    half_dim = HD // 2
    inv_freq = 10000.0 ** (-jnp.arange(0, HD, 2, dtype=jnp.float32) / HD)
    angles = places[:, None, None] * inv_freq[None, None, :]
    cosine = jnp.cos(angles)
    sine = jnp.sin(angles)
    lower = field[..., :half_dim].astype(jnp.float32)
    upper = field[..., half_dim:].astype(jnp.float32)
    return jnp.concatenate(
        [lower * cosine - upper * sine, upper * cosine + lower * sine], axis=-1
    ).astype(jnp.bfloat16)


def banded(field, blocks):
    framed = field.reshape((blocks + 2, WINDOW) + field.shape[1:])
    return jnp.concatenate([framed[:-2], framed[1:-1], framed[2:]], axis=1)


def rms_scale(field, gain_vec):
    return field * lax.rsqrt(jnp.mean(field * field, axis=-1, keepdims=True) + 1e-06) * gain_vec


def body(
    queries,
    key_heads,
    value_heads,
    sink_logit,
    doc_ids,
    residual,
    out_proj,
    gain_mix,
    up_proj,
    down_proj,
    gain_ffn_in,
    gain_ffn_out,
):
    tok_count = queries.shape[0]
    blocks = tok_count // WINDOW
    share_rows = tok_count // lax.axis_size("tp")
    q_local = queries.shape[1] // HD
    kv_local = key_heads.shape[1] // HD
    group_size = q_local // kv_local
    offset = lax.axis_index("sp") * tok_count
    up, down, up_near, down_near = start_weights(up_proj, down_proj)
    places = (offset + jnp.arange(tok_count)).astype(jnp.float32)
    rotated_q = rotate(queries.reshape(tok_count, q_local, HD), places).reshape(
        blocks, WINDOW, kv_local, group_size, HD
    )
    rotated_k = rotate(key_heads.reshape(tok_count, kv_local, HD), places).reshape(
        tok_count, kv_local * HD
    )
    rimmed = padded(jnp.stack([rotated_k, value_heads]), (("sp", 1),), WINDOW)
    key_win = banded(rimmed[0].reshape(-1, kv_local, HD), blocks)
    val_win = banded(rimmed[1].reshape(-1, kv_local, HD), blocks)
    padded_docs = jnp.pad(doc_ids, (WINDOW, WINDOW), constant_values=-1)
    key_docs = banded(lax.dynamic_slice_in_dim(padded_docs, offset, tok_count + 2 * WINDOW), blocks)
    query_docs = lax.dynamic_slice_in_dim(doc_ids, offset, tok_count).reshape(blocks, WINDOW)
    q_index = jnp.arange(WINDOW)[:, None]
    k_index = jnp.arange(3 * WINDOW)[None, :]
    in_window = jnp.abs(k_index - WINDOW - q_index) <= WINDOW
    allowed = (in_window[None] & (query_docs[:, :, None] == key_docs[:, None, :]))[:, None, None]
    scores = jnp.einsum(
        "nqkgd,nskd->nkgqs", rotated_q, key_win, preferred_element_type=jnp.float32
    ) * HD ** (-0.5)
    masked = jnp.where(allowed, scores, -1e30)
    sink_col = sink_logit.reshape(kv_local, group_size)[None, :, :, None]
    top_score = jnp.maximum(jnp.max(masked, axis=-1), sink_col)
    exp_scores = jnp.where(allowed, jnp.exp(masked - top_score[..., None]), 0.0)
    denom_sum = jnp.sum(exp_scores, axis=-1) + jnp.exp(sink_col - top_score)
    probs = (exp_scores / denom_sum[..., None]).astype(jnp.bfloat16)
    attn = (
        jnp.einsum("nkgqs,nskd->nqkgd", probs, val_win, preferred_element_type=jnp.float32)
        .astype(jnp.bfloat16)
        .reshape(tok_count, q_local * HD)
    )
    partial_mix = jnp.dot(attn, out_proj, preferred_element_type=jnp.float32).astype(jnp.bfloat16)
    mixed = summed_on_arrival(partial_mix, "tp", 0)
    own_resid = lax.dynamic_slice_in_dim(residual, lax.axis_index("tp") * share_rows, share_rows, 0)
    after_mix = (own_resid.astype(jnp.float32) + rms_scale(mixed, gain_mix)).astype(jnp.bfloat16)
    own_normed = rms_scale(after_mix.astype(jnp.float32), gain_ffn_in).astype(jnp.bfloat16)
    up_whole, down_whole = finish_weights(up, down, up_near, down_near)
    normed = collect(own_normed, "tp", 0)
    up_acts = jnp.dot(normed, up_whole, preferred_element_type=jnp.float32)
    hidden = jnp.square(jax.nn.relu(up_acts)).astype(jnp.bfloat16)
    ffn_out = summed_on_arrival(
        lax.dot_general(
            hidden, down_whole, (((1,), (1,)), ((), ())), preferred_element_type=jnp.float32
        ).astype(jnp.bfloat16),
        "tp",
        0,
    )
    return (after_mix.astype(jnp.float32) + rms_scale(ffn_out, gain_ffn_out)).astype(jnp.bfloat16)


def solution(mesh):
    return jax.shard_map(
        body,
        mesh=mesh,
        in_specs=(
            P("sp", "tp"),
            P("sp", "tp"),
            P("sp", "tp"),
            P("tp"),
            P(),
            P("sp", None),
            P("tp", None),
            P(),
            P("sp", "tp"),
            P("tp", "sp"),
            P(),
            P(),
        ),
        out_specs=P(("sp", "tp"), None),
        check_vma=False,
    )
```

profile of v0, /device:TPU:1, one launch (start us, length us, event | category | flops | bytes accessed | tf_op | source)
XLA Modules:
  0.0 223.7 jit_solution(10899430865978458654)
XLA Ops:
  0.0 1.9 fusion.29
  1.9 0.9 pad_maximum_fusion.11
  2.8 4.0 %collective-permute-start = (bf16[2,128,128]{2,1,0:T(8,128)(2,1)S(1)}, bf16[2,128,128]{2,1,0:T(8,128)(2,1)S(1)}, u32[]{:S(2)}, u32[]{:S(2)}) collective-permute-start(bf16[2,128,128]{2,1,0:T(8,128)(2,1)S(1)} %get-tuple-element.21), channel_id=1, source_target_pairs={{0,8},{8,16},{16,24},{24,32},{32,40},{40,48},{48,56},{56,64},{64,7... | collective-permute-start | bytes 196616 | tf_op jit(solution)/shard_map/ppermute | solution.py:84
  6.9 1.3 collective-permute-start.1
  8.2 0.4 multiply_cosine_fusion.1
  8.6 0.8 pad_dynamic-slice_fusion
  9.4 0.8 dynamic-slice_bitcast_fusion
  10.3 1.1 copy.58
  12.5 0.4 fusion.42
  13.8 0.4 fusion.2
  14.4 1.7 convolution_convert_fusion.1
  16.1 8.4 %all-to-all-start = ((bf16[8,48,2048]{2,1,0:T(8,128)(2,1)}), bf16[8,48,2048]{2,1,0:T(8,128)(2,1)S(1)}, u32[]{:S(2)}, u32[]{:S(2)}) async-start(bf16[8,48,2048]{2,1,0:T(8,128)(2,1)} %bitcast.130), calls=%async_computation | async-start | bytes 3145728 | tf_op jit(solution)/shard_map/all_to_all | solution.py:97
  24.6 20.6 %all-to-all-done = bf16[8,48,2048]{2,1,0:T(8,128)(2,1)S(1)} async-done(((bf16[8,48,2048]{2,1,0:T(8,128)(2,1)}), bf16[8,48,2048]{2,1,0:T(8,128)(2,1)S(1)}, u32[]{:S(2)}, u32[]{:S(2)}) %all-to-all-start) | async-done | bytes 1572896 | tf_op jit(solution)/shard_map/all_to_all | solution.py:97
  45.2 0.9 broadcast_in_dim.119
  46.0 16.3 %all-to-all-start.2 = ((bf16[4,2,32,1024]{3,2,1,0:T(8,128)(2,1)}), bf16[4,2,32,1024]{3,2,1,0:T(8,128)(2,1)S(1)}, u32[]{:S(2)}, u32[]{:S(2)}) async-start(bf16[4,2,32,1024]{3,2,1,0:T(8,128)(2,1)} %broadcast_in_dim.119), calls=%async_computation.2 | async-start | bytes 1048576 | tf_op jit(solution)/shard_map/all_to_all | solution.py:32
  62.7 1.2 fusion.6
  63.9 26.7 %all-to-all-done.2 = bf16[4,2,32,1024]{3,2,1,0:T(8,128)(2,1)S(1)} async-done(((bf16[4,2,32,1024]{3,2,1,0:T(8,128)(2,1)}), bf16[4,2,32,1024]{3,2,1,0:T(8,128)(2,1)S(1)}, u32[]{:S(2)}, u32[]{:S(2)}) %all-to-all-start.2) | async-done | bytes 524320 | tf_op jit(solution)/shard_map/all_to_all | solution.py:32
  90.6 0.9 slice_bitcast_fusion.1
  91.4 1.9 collective-permute-start.2
  93.5 1.4 broadcast_in_dim.118
  94.9 5.8 %all-to-all-start.1 = ((bf16[8,48,2048]{2,1,0:T(8,128)(2,1)}), bf16[8,48,2048]{2,1,0:T(8,128)(2,1)S(1)}, u32[]{:S(2)}, u32[]{:S(2)}) async-start(bf16[8,48,2048]{2,1,0:T(8,128)(2,1)} %broadcast_in_dim.118), calls=%async_computation.1 | async-start | bytes 3145728 | tf_op jit(solution)/shard_map/all_to_all | solution.py:109
  100.7 3.6 %collective-permute-start.3 = (bf16[4,32,1024]{2,1,0:T(8,128)(2,1)}, bf16[4,32,1024]{2,1,0:T(8,128)(2,1)S(1)}, u32[]{:S(2)}, u32[]{:S(2)}) collective-permute-start(bf16[4,32,1024]{2,1,0:T(8,128)(2,1)} %get-tuple-element.9), channel_id=1, source_target_pairs={{24,0},{0,8},{8,16},{16,24},{56,32},{32,40},{40,48},{48,56},{88,64... | collective-permute-start | bytes 786440 | tf_op jit(solution)/shard_map/ppermute | solution.py:14
  104.3 1.9 collective-permute-start.4
  106.2 4.9 %collective-permute-start.9 = (bf16[4,32,1024]{2,1,0:T(8,128)(2,1)}, bf16[4,32,1024]{2,1,0:T(8,128)(2,1)S(1)}, u32[]{:S(2)}, u32[]{:S(2)}) collective-permute-start(bf16[4,32,1024]{2,1,0:T(8,128)(2,1)} %get-tuple-element.10), channel_id=1, source_target_pairs={{32,0},{40,8},{48,16},{56,24},{64,32},{72,40},{80,48},{88,56},{96,... | collective-permute-start | bytes 786440 | tf_op jit(solution)/shard_map/ppermute | solution.py:14
  111.1 1.9 collective-permute-start.10
  113.1 3.2 %collective-permute-start.11 = (bf16[2,32,1024]{2,1,0:T(8,128)(2,1)S(1)}, bf16[2,32,1024]{2,1,0:T(8,128)(2,1)S(1)}, u32[]{:S(2)}, u32[]{:S(2)}) collective-permute-start(bf16[2,32,1024]{2,1,0:T(8,128)(2,1)S(1)} %get-tuple-element.12), channel_id=1, source_target_pairs={{64,0},{72,8},{80,16},{88,24},{96,32},{104,40},{112,48},{120,56},{... | collective-permute-start | bytes 393224 | tf_op jit(solution)/shard_map/ppermute | solution.py:14
  116.3 1.1 broadcast_in_dim.121
  117.4 1.0 bitcast_dynamic-update-slice_fusion.9
  118.4 3.5 %collective-permute-start.12 = (bf16[2,32,1024]{2,1,0:T(8,128)(2,1)S(1)}, bf16[2,32,1024]{2,1,0:T(8,128)(2,1)S(1)}, u32[]{:S(2)}, u32[]{:S(2)}) collective-permute-start(bf16[2,32,1024]{2,1,0:T(8,128)(2,1)S(1)} %get-tuple-element.11), channel_id=1, source_target_pairs={{448,0},{456,8},{464,16},{472,24},{480,32},{488,40},{496,48},{504,... | collective-permute-start | bytes 393224 | tf_op jit(solution)/shard_map/ppermute | solution.py:14
  121.9 5.4 %collective-permute-start.5 = (bf16[4,4,32,1024]{3,2,1,0:T(8,128)(2,1)S(1)}, bf16[4,4,32,1024]{3,2,1,0:T(8,128)(2,1)S(1)}, u32[]{:S(2)}, u32[]{:S(2)}) collective-permute-start(bf16[4,4,32,1024]{3,2,1,0:T(8,128)(2,1)S(1)} %bitcast_dynamic-update-slice_fusion.11), channel_id=1, source_target_pairs={{32,0},{40,8},{48,16},{56,24},{64,32},{72,40},{80,48},{88,56},{96,... | collective-permute-start | bytes 3145736 | tf_op jit(solution)/shard_map/ppermute | solution.py:14
  127.4 1.9 collective-permute-start.6
  129.6 3.7 %collective-permute-start.13 = (bf16[4,4,32,1024]{3,2,1,0:T(8,128)(2,1)S(1)}, bf16[4,4,32,1024]{3,2,1,0:T(8,128)(2,1)S(1)}, u32[]{:S(2)}, u32[]{:S(2)}) collective-permute-start(bf16[4,4,32,1024]{3,2,1,0:T(8,128)(2,1)S(1)} %bitcast_dynamic-update-slice_fusion.12), channel_id=1, source_target_pairs={{8,0},{16,8},{24,16},{0,24},{40,32},{48,40},{56,48},{32,56},{72,64... | collective-permute-start | bytes 3145736 | tf_op jit(solution)/shard_map/ppermute | solution.py:14
  133.3 2.5 %collective-permute-start.14 = (bf16[4,4,32,1024]{3,2,1,0:T(8,128)(2,1)S(1)}, bf16[4,4,32,1024]{3,2,1,0:T(8,128)(2,1)S(1)}, u32[]{:S(2)}, u32[]{:S(2)}) collective-permute-start(bf16[4,4,32,1024]{3,2,1,0:T(8,128)(2,1)S(1)} %bitcast_dynamic-update-slice_fusion.12), channel_id=1, source_target_pairs={{24,0},{0,8},{8,16},{16,24},{56,32},{32,40},{40,48},{48,56},{88,64... | collective-permute-start | bytes 3145736 | tf_op jit(solution)/shard_map/ppermute | solution.py:14
  135.8 3.7 %collective-permute-start.15 = (bf16[4,4,32,1024]{3,2,1,0:T(8,128)(2,1)S(1)}, bf16[4,4,32,1024]{3,2,1,0:T(8,128)(2,1)S(1)}, u32[]{:S(2)}, u32[]{:S(2)}) collective-permute-start(bf16[4,4,32,1024]{3,2,1,0:T(8,128)(2,1)S(1)} %bitcast_dynamic-update-slice_fusion.12), channel_id=1, source_target_pairs={{16,0},{24,8},{0,16},{8,24},{48,32},{56,40},{32,48},{40,56},{80,64... | collective-permute-start | bytes 3145736 | tf_op jit(solution)/shard_map/ppermute | solution.py:14
  139.6 9.0 %collective-permute-done.5 = bf16[4,4,32,1024]{3,2,1,0:T(8,128)(2,1)S(1)} collective-permute-done((bf16[4,4,32,1024]{3,2,1,0:T(8,128)(2,1)S(1)}, bf16[4,4,32,1024]{3,2,1,0:T(8,128)(2,1)S(1)}, u32[]{:S(2)}, u32[]{:S(2)}) %collective-permute-start.5) | collective-permute-done | bytes 1048608 | tf_op jit(solution)/shard_map/ppermute | solution.py:14
  148.5 3.6 %collective-permute-start.7 = (bf16[2,4,32,1024]{3,2,1,0:T(8,128)(2,1)S(1)}, bf16[2,4,32,1024]{3,2,1,0:T(8,128)(2,1)S(1)}, u32[]{:S(2)}, u32[]{:S(2)}) collective-permute-start(bf16[2,4,32,1024]{3,2,1,0:T(8,128)(2,1)S(1)} %get-tuple-element.8), channel_id=1, source_target_pairs={{64,0},{72,8},{80,16},{88,24},{96,32},{104,40},{112,48},{120,56},{... | collective-permute-start | bytes 1572872 | tf_op jit(solution)/shard_map/ppermute | solution.py:14
  152.2 0.5 broadcast_in_dim.125
  153.1 2.3 %collective-permute-start.8 = (bf16[2,4,32,1024]{3,2,1,0:T(8,128)(2,1)S(1)}, bf16[2,4,32,1024]{3,2,1,0:T(8,128)(2,1)S(1)}, u32[]{:S(2)}, u32[]{:S(2)}) collective-permute-start(bf16[2,4,32,1024]{3,2,1,0:T(8,128)(2,1)S(1)} %get-tuple-element.7), channel_id=1, source_target_pairs={{448,0},{456,8},{464,16},{472,24},{480,32},{488,40},{496,48},{504,... | collective-permute-start | bytes 1572872 | tf_op jit(solution)/shard_map/ppermute | solution.py:14
  155.5 13.5 %collective-permute-done.7 = bf16[2,4,32,1024]{3,2,1,0:T(8,128)(2,1)S(1)} collective-permute-done((bf16[2,4,32,1024]{3,2,1,0:T(8,128)(2,1)S(1)}, bf16[2,4,32,1024]{3,2,1,0:T(8,128)(2,1)S(1)}, u32[]{:S(2)}, u32[]{:S(2)}) %collective-permute-start.7) | collective-permute-done | bytes 524320 | tf_op jit(solution)/shard_map/ppermute | solution.py:14
  169.1 3.0 %broadcast_in_dim.136 = bf16[4,4,4,32,1024]{4,3,2,1,0:T(8,128)(2,1)} broadcast(bf16[4,4,32,1024]{3,2,1,0:T(8,128)(2,1)S(1)} %bitcast_dynamic-update-slice_fusion.12), dimensions={0,1,3,4} | broadcast | bytes 5242880 | tf_op jit(solution)/shard_map/broadcast_in_dim | solution.py:19
  172.3 1.1 bitcast_dynamic-update-slice_fusion.1
  173.5 1.2 bitcast_dynamic-update-slice_fusion
  174.6 6.6 %collective-permute-done.15 = bf16[4,4,32,1024]{3,2,1,0:T(8,128)(2,1)S(1)} collective-permute-done((bf16[4,4,32,1024]{3,2,1,0:T(8,128)(2,1)S(1)}, bf16[4,4,32,1024]{3,2,1,0:T(8,128)(2,1)S(1)}, u32[]{:S(2)}, u32[]{:S(2)}) %collective-permute-start.15) | collective-permute-done | bytes 1048608 | tf_op jit(solution)/shard_map/ppermute | solution.py:14
  181.2 1.1 bitcast_dynamic-update-slice_fusion.4
  182.3 8.1 %convolution_convert_fusion = bf16[384,2048]{1,0:T(8,128)(2,1)} fusion(bf16[2048,1024]{1,0:T(8,128)(2,1)} %bitcast.58, bf16[384,2048]{1,0:T(8,128)(2,1)S(1)} %bitcast.132, bf16[2048,1024]{1,0:T(8,128)(2,1)} %bitcast.131), kind=kOutput, calls=%fused_computation.2 | convolution fusion | flops 3223191552 | bytes 11534336 | tf_op jit(solution)/shard_map/dot_general | solution.py:203
  190.4 31.8 %all_to_all.20 = bf16[8,48,2048]{2,1,0:T(8,128)(2,1)S(1)} all-to-all(bf16[8,48,2048]{2,1,0:T(8,128)(2,1)} %bitcast.133), channel_id=1, replica_groups=mesh['sp'=64,'tp'=8] {'tp'}, dimensions={0} | all-to-all | bytes 3145728 | tf_op jit(solution)/shard_map/all_to_all | solution.py:97
  222.6 0.3 copy-done.7
  222.9 0.8 fusion.9
  (75 shorter events, 4.3 us)
Async XLA Ops:
  0.0 14.4 %copy-start = (bf16[256,2048]{1,0:T(8,128)(2,1)S(1)}, bf16[256,2048]{1,0:T(8,128)(2,1)}, u32[]{:S(2)}) copy-start(bf16[256,2048]{1,0:T(8,128)(2,1)} %param.18) | copy-start | bytes 3145732
  1.9 10.3 %copy-start.3 = (bf16[384,128]{1,0:T(8,128)(2,1)S(1)}, bf16[384,128]{1,0:T(8,128)(2,1)}, u32[]{:S(2)}) copy-start(bf16[384,128]{1,0:T(8,128)(2,1)} %param.14) | copy-start | bytes 294916
  2.8 9.5 %collective-permute-start = (bf16[2,128,128]{2,1,0:T(8,128)(2,1)S(1)}, bf16[2,128,128]{2,1,0:T(8,128)(2,1)S(1)}, u32[]{:S(2)}, u32[]{:S(2)}) collective-permute-start(bf16[2,128,128]{2,1,0:T(8,128)(2,1)S(1)} %get-tuple-element.21), channel_id=1, source_target_pairs={{0,8},{8,16},{16,24},{24,32},{32,40},{40,48},{48,56},{56,64},{64,7... | collective-permute-start | bytes 196616 | tf_op jit(solution)/shard_map/ppermute | solution.py:84
  6.9 5.4 %collective-permute-start.1 = (bf16[2,128,128]{2,1,0:T(8,128)(2,1)S(1)}, bf16[2,128,128]{2,1,0:T(8,128)(2,1)S(1)}, u32[]{:S(2)}, u32[]{:S(2)}) collective-permute-start(bf16[2,128,128]{2,1,0:T(8,128)(2,1)S(1)} %get-tuple-element.22), channel_id=1, source_target_pairs={{8,0},{16,8},{24,16},{32,24},{40,32},{48,40},{56,48},{64,56},{72,6... | collective-permute-start | bytes 196616 | tf_op jit(solution)/shard_map/ppermute | solution.py:85
  12.4 0.7 copy-start.9
  16.1 8.4 %copy-start.4 = (bf16[1024,32]{0,1:T(8,128)(2,1)S(1)}, bf16[1024,32]{0,1:T(8,128)(2,1)}, u32[]{:S(2)}) copy-start(bf16[1024,32]{0,1:T(8,128)(2,1)} %param.21) | copy-start | bytes 196612
  16.1 8.4 %copy-start.5 = (bf16[32,1024]{1,0:T(8,128)(2,1)S(1)}, bf16[32,1024]{1,0:T(8,128)(2,1)}, u32[]{:S(2)}) copy-start(bf16[32,1024]{1,0:T(8,128)(2,1)} %param.20) | copy-start | bytes 196612
  16.1 29.0 %all-to-all-start = ((bf16[8,48,2048]{2,1,0:T(8,128)(2,1)}), bf16[8,48,2048]{2,1,0:T(8,128)(2,1)S(1)}, u32[]{:S(2)}, u32[]{:S(2)}) async-start(bf16[8,48,2048]{2,1,0:T(8,128)(2,1)} %bitcast.130), calls=%async_computation | async-start | bytes 3145728 | tf_op jit(solution)/shard_map/all_to_all | solution.py:97
  46.0 16.6 %copy-start.6 = (f32[2048]{0:T(1024)S(1)}, f32[2048]{0:T(1024)}, u32[]{:S(2)}) copy-start(f32[2048]{0:T(1024)} %param.19) | copy-start | bytes 24580
  46.0 44.5 %all-to-all-start.2 = ((bf16[4,2,32,1024]{3,2,1,0:T(8,128)(2,1)}), bf16[4,2,32,1024]{3,2,1,0:T(8,128)(2,1)S(1)}, u32[]{:S(2)}, u32[]{:S(2)}) async-start(bf16[4,2,32,1024]{3,2,1,0:T(8,128)(2,1)} %broadcast_in_dim.119), calls=%async_computation.2 | async-start | bytes 1048576 | tf_op jit(solution)/shard_map/all_to_all | solution.py:32
  62.5 30.8 %copy-start.8 = (f32[2048]{0:T(1024)S(1)}, f32[2048]{0:T(1024)}, u32[]{:S(2)}) copy-start(f32[2048]{0:T(1024)} %param.22) | copy-start | bytes 24580
  91.4 21.7 %collective-permute-start.2 = (bf16[4,32,1024]{2,1,0:T(8,128)(2,1)}, bf16[4,32,1024]{2,1,0:T(8,128)(2,1)}, u32[]{:S(2)}, u32[]{:S(2)}) collective-permute-start(bf16[4,32,1024]{2,1,0:T(8,128)(2,1)} %get-tuple-element.9), channel_id=1, source_target_pairs={{8,0},{16,8},{24,16},{0,24},{40,32},{48,40},{56,48},{32,56},{72,64... | collective-permute-start | bytes 786440 | tf_op jit(solution)/shard_map/ppermute | solution.py:14
  94.9 87.4 %all-to-all-start.1 = ((bf16[8,48,2048]{2,1,0:T(8,128)(2,1)}), bf16[8,48,2048]{2,1,0:T(8,128)(2,1)S(1)}, u32[]{:S(2)}, u32[]{:S(2)}) async-start(bf16[8,48,2048]{2,1,0:T(8,128)(2,1)} %broadcast_in_dim.118), calls=%async_computation.1 | async-start | bytes 3145728 | tf_op jit(solution)/shard_map/all_to_all | solution.py:109
  100.7 17.7 %collective-permute-start.3 = (bf16[4,32,1024]{2,1,0:T(8,128)(2,1)}, bf16[4,32,1024]{2,1,0:T(8,128)(2,1)S(1)}, u32[]{:S(2)}, u32[]{:S(2)}) collective-permute-start(bf16[4,32,1024]{2,1,0:T(8,128)(2,1)} %get-tuple-element.9), channel_id=1, source_target_pairs={{24,0},{0,8},{8,16},{16,24},{56,32},{32,40},{40,48},{48,56},{88,64... | collective-permute-start | bytes 786440 | tf_op jit(solution)/shard_map/ppermute | solution.py:14
  104.3 17.6 %collective-permute-start.4 = (bf16[4,32,1024]{2,1,0:T(8,128)(2,1)}, bf16[4,32,1024]{2,1,0:T(8,128)(2,1)S(1)}, u32[]{:S(2)}, u32[]{:S(2)}) collective-permute-start(bf16[4,32,1024]{2,1,0:T(8,128)(2,1)} %get-tuple-element.9), channel_id=1, source_target_pairs={{16,0},{24,8},{0,16},{8,24},{48,32},{56,40},{32,48},{40,56},{80,64... | collective-permute-start | bytes 786440 | tf_op jit(solution)/shard_map/ppermute | solution.py:14
  106.2 21.1 %collective-permute-start.9 = (bf16[4,32,1024]{2,1,0:T(8,128)(2,1)}, bf16[4,32,1024]{2,1,0:T(8,128)(2,1)S(1)}, u32[]{:S(2)}, u32[]{:S(2)}) collective-permute-start(bf16[4,32,1024]{2,1,0:T(8,128)(2,1)} %get-tuple-element.10), channel_id=1, source_target_pairs={{32,0},{40,8},{48,16},{56,24},{64,32},{72,40},{80,48},{88,56},{96,... | collective-permute-start | bytes 786440 | tf_op jit(solution)/shard_map/ppermute | solution.py:14
  111.1 18.3 %collective-permute-start.10 = (bf16[4,32,1024]{2,1,0:T(8,128)(2,1)}, bf16[4,32,1024]{2,1,0:T(8,128)(2,1)S(1)}, u32[]{:S(2)}, u32[]{:S(2)}) collective-permute-start(bf16[4,32,1024]{2,1,0:T(8,128)(2,1)} %get-tuple-element.10), channel_id=1, source_target_pairs={{480,0},{488,8},{496,16},{504,24},{0,32},{8,40},{16,48},{24,56},{3... | collective-permute-start | bytes 786440 | tf_op jit(solution)/shard_map/ppermute | solution.py:14
  113.1 16.2 %copy-start.2 = (bf16[4,32,1024]{2,1,0:T(8,128)(2,1)S(1)}, bf16[4,32,1024]{2,1,0:T(8,128)(2,1)}, u32[]{:S(2)}) copy-start(bf16[4,32,1024]{2,1,0:T(8,128)(2,1)} %get-tuple-element.10) | copy-start | bytes 786436
  113.1 16.4 %collective-permute-start.11 = (bf16[2,32,1024]{2,1,0:T(8,128)(2,1)S(1)}, bf16[2,32,1024]{2,1,0:T(8,128)(2,1)S(1)}, u32[]{:S(2)}, u32[]{:S(2)}) collective-permute-start(bf16[2,32,1024]{2,1,0:T(8,128)(2,1)S(1)} %get-tuple-element.12), channel_id=1, source_target_pairs={{64,0},{72,8},{80,16},{88,24},{96,32},{104,40},{112,48},{120,56},{... | collective-permute-start | bytes 393224 | tf_op jit(solution)/shard_map/ppermute | solution.py:14
  118.4 11.2 %collective-permute-start.12 = (bf16[2,32,1024]{2,1,0:T(8,128)(2,1)S(1)}, bf16[2,32,1024]{2,1,0:T(8,128)(2,1)S(1)}, u32[]{:S(2)}, u32[]{:S(2)}) collective-permute-start(bf16[2,32,1024]{2,1,0:T(8,128)(2,1)S(1)} %get-tuple-element.11), channel_id=1, source_target_pairs={{448,0},{456,8},{464,16},{472,24},{480,32},{488,40},{496,48},{504,... | collective-permute-start | bytes 393224 | tf_op jit(solution)/shard_map/ppermute | solution.py:14
  121.9 26.6 %collective-permute-start.5 = (bf16[4,4,32,1024]{3,2,1,0:T(8,128)(2,1)S(1)}, bf16[4,4,32,1024]{3,2,1,0:T(8,128)(2,1)S(1)}, u32[]{:S(2)}, u32[]{:S(2)}) collective-permute-start(bf16[4,4,32,1024]{3,2,1,0:T(8,128)(2,1)S(1)} %bitcast_dynamic-update-slice_fusion.11), channel_id=1, source_target_pairs={{32,0},{40,8},{48,16},{56,24},{64,32},{72,40},{80,48},{88,56},{96,... | collective-permute-start | bytes 3145736 | tf_op jit(solution)/shard_map/ppermute | solution.py:14
  127.4 25.7 %collective-permute-start.6 = (bf16[4,4,32,1024]{3,2,1,0:T(8,128)(2,1)S(1)}, bf16[4,4,32,1024]{3,2,1,0:T(8,128)(2,1)S(1)}, u32[]{:S(2)}, u32[]{:S(2)}) collective-permute-start(bf16[4,4,32,1024]{3,2,1,0:T(8,128)(2,1)S(1)} %bitcast_dynamic-update-slice_fusion.11), channel_id=1, source_target_pairs={{480,0},{488,8},{496,16},{504,24},{0,32},{8,40},{16,48},{24,56},{3... | collective-permute-start | bytes 3145736 | tf_op jit(solution)/shard_map/ppermute | solution.py:14
  129.6 39.5 %collective-permute-start.13 = (bf16[4,4,32,1024]{3,2,1,0:T(8,128)(2,1)S(1)}, bf16[4,4,32,1024]{3,2,1,0:T(8,128)(2,1)S(1)}, u32[]{:S(2)}, u32[]{:S(2)}) collective-permute-start(bf16[4,4,32,1024]{3,2,1,0:T(8,128)(2,1)S(1)} %bitcast_dynamic-update-slice_fusion.12), channel_id=1, source_target_pairs={{8,0},{16,8},{24,16},{0,24},{40,32},{48,40},{56,48},{32,56},{72,64... | collective-permute-start | bytes 3145736 | tf_op jit(solution)/shard_map/ppermute | solution.py:14
  133.3 40.2 %collective-permute-start.14 = (bf16[4,4,32,1024]{3,2,1,0:T(8,128)(2,1)S(1)}, bf16[4,4,32,1024]{3,2,1,0:T(8,128)(2,1)S(1)}, u32[]{:S(2)}, u32[]{:S(2)}) collective-permute-start(bf16[4,4,32,1024]{3,2,1,0:T(8,128)(2,1)S(1)} %bitcast_dynamic-update-slice_fusion.12), channel_id=1, source_target_pairs={{24,0},{0,8},{8,16},{16,24},{56,32},{32,40},{40,48},{48,56},{88,64... | collective-permute-start | bytes 3145736 | tf_op jit(solution)/shard_map/ppermute | solution.py:14
  135.8 45.5 %collective-permute-start.15 = (bf16[4,4,32,1024]{3,2,1,0:T(8,128)(2,1)S(1)}, bf16[4,4,32,1024]{3,2,1,0:T(8,128)(2,1)S(1)}, u32[]{:S(2)}, u32[]{:S(2)}) collective-permute-start(bf16[4,4,32,1024]{3,2,1,0:T(8,128)(2,1)S(1)} %bitcast_dynamic-update-slice_fusion.12), channel_id=1, source_target_pairs={{16,0},{24,8},{0,16},{8,24},{48,32},{56,40},{32,48},{40,56},{80,64... | collective-permute-start | bytes 3145736 | tf_op jit(solution)/shard_map/ppermute | solution.py:14
  148.5 20.4 %collective-permute-start.7 = (bf16[2,4,32,1024]{3,2,1,0:T(8,128)(2,1)S(1)}, bf16[2,4,32,1024]{3,2,1,0:T(8,128)(2,1)S(1)}, u32[]{:S(2)}, u32[]{:S(2)}) collective-permute-start(bf16[2,4,32,1024]{3,2,1,0:T(8,128)(2,1)S(1)} %get-tuple-element.8), channel_id=1, source_target_pairs={{64,0},{72,8},{80,16},{88,24},{96,32},{104,40},{112,48},{120,56},{... | collective-permute-start | bytes 1572872 | tf_op jit(solution)/shard_map/ppermute | solution.py:14
  153.1 15.9 %collective-permute-start.8 = (bf16[2,4,32,1024]{3,2,1,0:T(8,128)(2,1)S(1)}, bf16[2,4,32,1024]{3,2,1,0:T(8,128)(2,1)S(1)}, u32[]{:S(2)}, u32[]{:S(2)}) collective-permute-start(bf16[2,4,32,1024]{3,2,1,0:T(8,128)(2,1)S(1)} %get-tuple-element.7), channel_id=1, source_target_pairs={{448,0},{456,8},{464,16},{472,24},{480,32},{488,40},{496,48},{504,... | collective-permute-start | bytes 1572872 | tf_op jit(solution)/shard_map/ppermute | solution.py:14
  169.1 3.2 %copy-start.1 = (bf16[4,4,4,32,1024]{4,3,2,1,0:T(8,128)(2,1)}, bf16[4,4,4,32,1024]{4,3,2,1,0:T(8,128)(2,1)S(1)}, u32[]{:S(2)}) copy-start(bf16[4,4,4,32,1024]{4,3,2,1,0:T(8,128)(2,1)S(1)} %bitcast_dynamic-update-slice_fusion.6) | copy-start | bytes 12582916
  222.2 0.7 copy-start.7
where the time goes:
time: 225 us; the launch traced here: 224 us
  starting transfers between devices  79.8 us (35%)
  waiting for transfers between devices  76.6 us (34%)
  blocking collectives  31.8 us (14%)
  local copies, waits for them, and re-layouts  17.2 us (8%)
  matrix products  10.7 us (5%)
  other arithmetic  7.02 us (3%)
    ppermute x14, starting transfers between devices, fetch(): return lax.ppermute(shard, 'sp', pairs)  44 us
    all_to_all x1, blocking collectives, summed_on_arrival(): lax.all_to_all(pieces, axis, split_axis=0, concat_axis=0, tiled=True)  31.8 us
    ppermute x14, waiting for transfers between devices, fetch(): return lax.ppermute(shard, 'sp', pairs)  29.3 us
    all_to_all x1, waiting for transfers between devices, far_stage(): lax.all_to_all(spread, 'sp', 0, 0, axis_index_groups=groups, tiled=True)  26.7 us
    all_to_all x1, waiting for transfers between devices, summed_on_arrival(): lax.all_to_all(pieces, axis, split_axis=0, concat_axis=0, tiled=True)  20.6 us
    all_to_all x1, starting transfers between devices, far_stage(): lax.all_to_all(spread, 'sp', 0, 0, axis_index_groups=groups, tiled=True)  16.3 us
    all_to_all x1, starting transfers between devices, summed_on_arrival(): lax.all_to_all(pieces, axis, split_axis=0, concat_axis=0, tiled=True)  8.43 us
    dot_general x1, matrix products, body(): lax.dot_general(hidden, down_whole, (((1,), (1,)), ((), ())), preferred_e...  8.08 us
  transfers between devices with their start and end apart: 19, of which 6 were waited for; matrix products, arithmetic and copies ran while one was open for 7% of the time, Pallas kernels for 0%

commit v1 on v0

--- a/solution.py
+++ b/solution.py
@@ -1,3 +1,5 @@
+import itertools
+
 import jax
 import jax.numpy as jnp
 from jax import lax
@@ -50,28 +52,64 @@
     return placed(shard, pieces, dim, own_at)
 
 
-def joined_y(shard, near, far, dim, own_at):
-    pieces = [(near[0], 1, 0, 0), (near[1], 3, 0, 0), (far, 2, 0, 0)]
-    return placed(shard, pieces, dim, own_at)
+def joined_y(shard, other, dim, own_at):
+    whole = jnp.expand_dims(shard, dim)
+    whole = jnp.broadcast_to(whole, (*whole.shape[:dim], 2, *whole.shape[dim + 1 :]))
+    at = [0] * whole.ndim
+    at[dim] = 1 - own_at
+    return lax.dynamic_update_slice(whole, jnp.expand_dims(other, dim), at)
+
+
+def device(z, y, x, core):
+    return (4 * z + y) * 8 + 2 * x + core
+
+
+def paired(shard):
+    pairs = []
+    for z, y, x, core in itertools.product(range(16), range(4), range(4), range(2)):
+        own = device(z, y, x, core)
+        pairs.append((own, own if core == y % 2 else device(z, y ^ 1, x, 1 - core)))
+    return lax.ppermute(shard, ("sp", "tp"), pairs)
+
+
+def swapped(shard):
+    return lax.ppermute(shard, "tp", [(i, i ^ 1) for i in range(8)])
+
+
+def token_groups():
+    return [
+        [device(z, 2 * q + par, x, core) for par in range(2) for x in range(4)]
+        for z in range(16)
+        for q in range(2)
+        for core in range(2)
+    ]
+
+
+def exchanged(pieces):
+    return lax.all_to_all(
+        pieces, ("sp", "tp"), 0, 0, axis_index_groups=token_groups(), tiled=True
+    )
+
+
+def halves(field, core):
+    first, second = (field[:, 0], field[:, 1])
+    return jnp.where(core == 0, first, second), jnp.where(core == 0, second, first)
 
 
 def start_weights(up_proj, down_proj):
     place = lax.axis_index("sp")
     z, y = (place // 4, place % 4)
-    far = far_stage(jnp.stack([up_proj, down_proj.T]))
+    both = paired(jnp.stack([up_proj, down_proj.T]))
+    far = far_stage(both)
     up, down = (far[:, 0], far[:, 1])
-    up = joined_y(up, beside(up, "y"), fetch(up, 0, 2), 1, y)
-    down = joined_z(down, beside(down, "z"), across_z(down), 1, z % 4)
-    return up, down, beside(up, "z"), beside(down, "y")
-
-
-def finish_weights(up, down, up_near, down_near):
-    place = lax.axis_index("sp")
-    z, y = (place // 4, place % 4)
-    up_far, down_far = (across_z(up), fetch(down, 0, 2))
-    up_whole = joined_z(up, up_near, up_far, 1, z % 4)
-    down_whole = joined_y(down, down_near, down_far, 2, y)
-    return up_whole.reshape(2048, -1), down_whole.reshape(2048, -1)
+    up_other = fetch(up, 0, 2)
+    down_near, down_far = (beside(down, "z"), across_z(down))
+    up = joined_y(up, up_other, 1, y // 2)
+    down = joined_z(down, down_near, down_far, 1, z % 4)
+    up_near, up_far, down_other = (beside(up, "z"), across_z(up), fetch(down, 0, 2))
+    up = joined_z(up, up_near, up_far, 1, z % 4).reshape(1024, 1024)
+    down = joined_y(down, down_other, 2, y // 2).reshape(1024, 1024)
+    return up, swapped(up), down, swapped(down)
 
 
 def padded(shard, sides, width):
@@ -96,23 +134,6 @@
     pieces = split_up(shard, dim, lax.axis_size(axis))
     arrived = lax.all_to_all(pieces, axis, split_axis=0, concat_axis=0, tiled=True)
     return arrived.astype(jnp.float32).sum(axis=0)
-
-
-def joined_along(pieces, dim):
-    pieces = jnp.moveaxis(pieces, 0, dim)
-    lengths = pieces.shape
-    return pieces.reshape(*lengths[:dim], lengths[dim] * lengths[dim + 1], *lengths[dim + 2 :])
-
-
-def copy_for_each(shard, axis):
-    devices = lax.axis_size(axis)
-    return lax.all_to_all(
-        jnp.broadcast_to(shard[None], (devices, *shard.shape)), axis, 0, 0, tiled=True
-    )
-
-
-def collect(shard, axis, dim):
-    return joined_along(copy_for_each(shard, axis), dim)
 
 
 def rotate(field, places):
@@ -158,7 +179,8 @@
     kv_local = key_heads.shape[1] // HD
     group_size = q_local // kv_local
     offset = lax.axis_index("sp") * tok_count
-    up, down, up_near, down_near = start_weights(up_proj, down_proj)
+    up, up_other, down, down_other = start_weights(up_proj, down_proj)
+    core = lax.axis_index("tp") % 2
     places = (offset + jnp.arange(tok_count)).astype(jnp.float32)
     rotated_q = rotate(queries.reshape(tok_count, q_local, HD), places).reshape(
         blocks, WINDOW, kv_local, group_size, HD
@@ -195,17 +217,22 @@
     own_resid = lax.dynamic_slice_in_dim(residual, lax.axis_index("tp") * share_rows, share_rows, 0)
     after_mix = (own_resid.astype(jnp.float32) + rms_scale(mixed, gain_mix)).astype(jnp.bfloat16)
     own_normed = rms_scale(after_mix.astype(jnp.float32), gain_ffn_in).astype(jnp.bfloat16)
-    up_whole, down_whole = finish_weights(up, down, up_near, down_near)
-    normed = collect(own_normed, "tp", 0)
-    up_acts = jnp.dot(normed, up_whole, preferred_element_type=jnp.float32)
+    first, second = halves(own_normed.reshape(-1, 32, 2, 32).swapaxes(1, 2), core)
+    ordered = jnp.concatenate([first.reshape(-1, 1024), second.reshape(-1, 1024)], axis=1)
+    normed = exchanged(jnp.broadcast_to(ordered[None], (8, *ordered.shape)))
+    normed = normed.reshape(-1, 2048)
+    up_acts = jnp.dot(normed[:, :1024], up, preferred_element_type=jnp.float32) + jnp.dot(
+        normed[:, 1024:], up_other, preferred_element_type=jnp.float32
+    )
     hidden = jnp.square(jax.nn.relu(up_acts)).astype(jnp.bfloat16)
-    ffn_out = summed_on_arrival(
-        lax.dot_general(
-            hidden, down_whole, (((1,), (1,)), ((), ())), preferred_element_type=jnp.float32
-        ).astype(jnp.bfloat16),
-        "tp",
-        0,
-    )
+    across = (((1,), (1,)), ((), ()))
+    parts = [
+        lax.dot_general(hidden, w, across, preferred_element_type=jnp.float32).astype(jnp.bfloat16)
+        for w in (down, down_other)
+    ]
+    arrived = exchanged(jnp.concatenate(parts, axis=1).reshape(8, -1, 2048))
+    summed = arrived.astype(jnp.float32).sum(axis=0).reshape(-1, 2, 32, 32)
+    ffn_out = jnp.stack(halves(summed, core), axis=2).reshape(-1, 2048)
     return (after_mix.astype(jnp.float32) + rms_scale(ffn_out, gain_ffn_out)).astype(jnp.bfloat16)
 
 

time: 225 us -> 211 us (0.938)
  waiting for transfers between devices: 76.6 us -> 63.7 us
  blocking collectives: 31.8 us -> 24.5 us
  matrix products: 10.7 us -> 13.5 us
    ppermute x14 -> x10, waiting for transfers between devices: 29.3 us -> 4.55 us  [fetch(): return lax.ppermute(shard, 'sp', pairs)]
    all_to_all x1, waiting for transfers between devices: 0.01 us -> 15.5 us  [exchanged(): lax.all_to_all(pieces, ('sp', 'tp'), 0, 0, axis_index_groups=token_groups...]
    ppermute x0 -> x3, starting transfers between devices: none -> 14.7 us  [the longest x2 11.1 us: swapped(): return lax.ppermute(shard, 'tp', [(i, i ^ 1) for i in range(8)])]
    ppermute x14 -> x10, starting transfers between devices: 44 us -> 31.8 us  [fetch(): return lax.ppermute(shard, 'sp', pairs)]
    all_to_all x1, blocking collectives: 31.8 us -> 24.5 us  [exchanged(): lax.all_to_all(pieces, ('sp', 'tp'), 0, 0, axis_index_groups=token_groups...]
    all_to_all x1, waiting for transfers between devices: 20.6 us -> 14 us  [summed_on_arrival(): lax.all_to_all(pieces, axis, split_axis=0, concat_axis=0, tiled=True)]
    broadcast_in_dim x5 -> x3, local copies, waits for them, and re-layouts: 5.57 us -> 1.8 us  [placed(): jnp.broadcast_to(whole, (*whole.shape[:dim], 4, *whole.shape[dim + 1:]))]
    ppermute x0 -> x3, waiting for transfers between devices: none -> 3 us  [the longest x1 3 us: paired(): return lax.ppermute(shard, ('sp', 'tp'), pairs)]
  transfers between devices with their start and end apart: 19 -> 18, of which waited for: 6 -> 6; matrix products, arithmetic and copies ran while one was open for 7% -> 12% of each run, Pallas kernels for 0% -> 0%
where the time goes in v1:
time: 211 us; the launch traced here: 208 us
  starting transfers between devices  81.4 us (39%)
  waiting for transfers between devices  63.7 us (30%)
  blocking collectives  24.5 us (12%)
  local copies, waits for them, and re-layouts  16.7 us (8%)
  matrix products  13.5 us (6%)
  other arithmetic  7.53 us (4%)
    ppermute x10, starting transfers between devices, fetch(): return lax.ppermute(shard, 'sp', pairs)  31.8 us
    all_to_all x1, waiting for transfers between devices, far_stage(): lax.all_to_all(spread, 'sp', 0, 0, axis_index_groups=groups, tiled=True)  26.7 us
    all_to_all x1, blocking collectives, exchanged(): lax.all_to_all(pieces, ('sp', 'tp'), 0, 0, axis_index_groups=token_groups...  24.5 us
    all_to_all x1, starting transfers between devices, far_stage(): lax.all_to_all(spread, 'sp', 0, 0, axis_index_groups=groups, tiled=True)  16.3 us
    all_to_all x1, waiting for transfers between devices, exchanged(): lax.all_to_all(pieces, ('sp', 'tp'), 0, 0, axis_index_groups=token_groups...  15.5 us
    all_to_all x1, waiting for transfers between devices, summed_on_arrival(): lax.all_to_all(pieces, axis, split_axis=0, concat_axis=0, tiled=True)  14 us
    ppermute x2, starting transfers between devices, swapped(): return lax.ppermute(shard, 'tp', [(i, i ^ 1) for i in range(8)])  11.1 us
    all_to_all x1, starting transfers between devices, summed_on_arrival(): lax.all_to_all(pieces, axis, split_axis=0, concat_axis=0, tiled=True)  8.43 us
  transfers between devices with their start and end apart: 18, of which 6 were waited for; matrix products, arithmetic and copies ran while one was open for 12% of the time, Pallas kernels for 0%

profile of v1, /device:TPU:1, one launch (start us, length us, event | category | flops | bytes accessed | tf_op | source)
XLA Modules:
  0.0 208.0 jit_solution(1475676945618550205)
XLA Ops:
  0.0 1.9 fusion.33
  1.9 0.9 pad_maximum_fusion.14
  2.8 4.0 %collective-permute-start = (bf16[2,128,128]{2,1,0:T(8,128)(2,1)S(1)}, bf16[2,128,128]{2,1,0:T(8,128)(2,1)S(1)}, u32[]{:S(2)}, u32[]{:S(2)}) collective-permute-start(bf16[2,128,128]{2,1,0:T(8,128)(2,1)S(1)} %get-tuple-element.25), channel_id=1, source_target_pairs={{0,8},{8,16},{16,24},{24,32},{32,40},{40,48},{48,56},{56,64},{64,7... | collective-permute-start | bytes 196616 | tf_op jit(solution)/shard_map/ppermute | solution.py:122
  6.9 1.3 collective-permute-start.1
  8.2 0.4 multiply_cosine_fusion.1
  8.6 1.1 copy.74
  9.7 0.8 pad_dynamic-slice_fusion
  10.5 0.8 dynamic-slice_bitcast_fusion
  12.5 0.4 fusion.45
  13.8 0.4 fusion.2
  14.4 1.7 convolution_convert_fusion
  16.1 8.4 %all-to-all-start = ((bf16[8,48,2048]{2,1,0:T(8,128)(2,1)}), bf16[8,48,2048]{2,1,0:T(8,128)(2,1)S(1)}, u32[]{:S(2)}, u32[]{:S(2)}) async-start(bf16[8,48,2048]{2,1,0:T(8,128)(2,1)} %bitcast.139), calls=%async_computation | async-start | bytes 3145728 | tf_op jit(solution)/shard_map/all_to_all | solution.py:135
  24.6 3.6 %collective-permute-start.2 = (bf16[2,32,1024]{2,1,0:T(8,128)(2,1)S(1)}, bf16[2,32,1024]{2,1,0:T(8,128)(2,1)S(1)}, u32[]{:S(2)}, u32[]{:S(2)}) collective-permute-start(bf16[2,32,1024]{2,1,0:T(8,128)(2,1)S(1)} %pad_maximum_fusion.3), channel_id=1, source_target_pairs={{0,0},{1,8},{2,2},{3,10},{4,4},{5,12},{6,6},{7,14},{8,1},{9,9},{10... | collective-permute-start | bytes 393224 | tf_op jit(solution)/shard_map/ppermute | solution.py:72
  28.2 3.0 %collective-permute-done.2 = bf16[2,32,1024]{2,1,0:T(8,128)(2,1)S(1)} collective-permute-done((bf16[2,32,1024]{2,1,0:T(8,128)(2,1)S(1)}, bf16[2,32,1024]{2,1,0:T(8,128)(2,1)S(1)}, u32[]{:S(2)}, u32[]{:S(2)}) %collective-permute-start.2) | collective-permute-done | bytes 131104 | tf_op jit(solution)/shard_map/ppermute | solution.py:72
  31.2 14.0 %all-to-all-done = bf16[8,48,2048]{2,1,0:T(8,128)(2,1)S(1)} async-done(((bf16[8,48,2048]{2,1,0:T(8,128)(2,1)}), bf16[8,48,2048]{2,1,0:T(8,128)(2,1)S(1)}, u32[]{:S(2)}, u32[]{:S(2)}) %all-to-all-start) | async-done | bytes 1572896 | tf_op jit(solution)/shard_map/all_to_all | solution.py:135
  45.2 0.9 broadcast_in_dim.107
  46.1 16.3 %all-to-all-start.2 = ((bf16[4,2,32,1024]{3,2,1,0:T(8,128)(2,1)}), bf16[4,2,32,1024]{3,2,1,0:T(8,128)(2,1)S(1)}, u32[]{:S(2)}, u32[]{:S(2)}) async-start(bf16[4,2,32,1024]{3,2,1,0:T(8,128)(2,1)} %broadcast_in_dim.107), calls=%async_computation.2 | async-start | bytes 1048576 | tf_op jit(solution)/shard_map/all_to_all | solution.py:34
  62.7 1.2 fusion.10
  63.9 26.7 %all-to-all-done.2 = bf16[4,2,32,1024]{3,2,1,0:T(8,128)(2,1)S(1)} async-done(((bf16[4,2,32,1024]{3,2,1,0:T(8,128)(2,1)}), bf16[4,2,32,1024]{3,2,1,0:T(8,128)(2,1)S(1)}, u32[]{:S(2)}, u32[]{:S(2)}) %all-to-all-start.2) | async-done | bytes 524320 | tf_op jit(solution)/shard_map/all_to_all | solution.py:34
  90.6 1.9 collective-permute-start.3
  92.5 3.1 %collective-permute-start.9 = (bf16[4,32,1024]{2,1,0:T(8,128)(2,1)S(1)}, bf16[4,32,1024]{2,1,0:T(8,128)(2,1)S(1)}, u32[]{:S(2)}, u32[]{:S(2)}) collective-permute-start(bf16[4,32,1024]{2,1,0:T(8,128)(2,1)S(1)} %get-tuple-element.11), channel_id=1, source_target_pairs={{32,0},{40,8},{48,16},{56,24},{64,32},{72,40},{80,48},{88,56},{96,... | collective-permute-start | bytes 786440 | tf_op jit(solution)/shard_map/ppermute | solution.py:16
  95.6 2.4 %collective-permute-start.10 = (bf16[4,32,1024]{2,1,0:T(8,128)(2,1)S(1)}, bf16[4,32,1024]{2,1,0:T(8,128)(2,1)S(1)}, u32[]{:S(2)}, u32[]{:S(2)}) collective-permute-start(bf16[4,32,1024]{2,1,0:T(8,128)(2,1)S(1)} %get-tuple-element.11), channel_id=1, source_target_pairs={{480,0},{488,8},{496,16},{504,24},{0,32},{8,40},{16,48},{24,56},{3... | collective-permute-start | bytes 786440 | tf_op jit(solution)/shard_map/ppermute | solution.py:16
  98.1 5.5 %collective-permute-start.11 = (bf16[2,32,1024]{2,1,0:T(8,128)(2,1)S(1)}, bf16[2,32,1024]{2,1,0:T(8,128)(2,1)S(1)}, u32[]{:S(2)}, u32[]{:S(2)}) collective-permute-start(bf16[2,32,1024]{2,1,0:T(8,128)(2,1)S(1)} %get-tuple-element.10), channel_id=1, source_target_pairs={{64,0},{72,8},{80,16},{88,24},{96,32},{104,40},{112,48},{120,56},{... | collective-permute-start | bytes 393224 | tf_op jit(solution)/shard_map/ppermute | solution.py:16
  103.6 1.9 collective-permute-start.12
  105.6 4.3 %collective-permute-start.4 = (bf16[4,2,32,1024]{3,2,1,0:T(8,128)(2,1)S(1)}, bf16[4,2,32,1024]{3,2,1,0:T(8,128)(2,1)S(1)}, u32[]{:S(2)}, u32[]{:S(2)}) collective-permute-start(bf16[4,2,32,1024]{3,2,1,0:T(8,128)(2,1)S(1)} %bitcast_dynamic-update-slice_fusion.7), channel_id=1, source_target_pairs={{32,0},{40,8},{48,16},{56,24},{64,32},{72,40},{80,48},{88,56},{96,... | collective-permute-start | bytes 1572872 | tf_op jit(solution)/shard_map/ppermute | solution.py:16
  109.9 1.9 collective-permute-start.5
  112.1 4.5 %collective-permute-start.6 = (bf16[2,2,32,1024]{3,2,1,0:T(8,128)(2,1)S(1)}, bf16[2,2,32,1024]{3,2,1,0:T(8,128)(2,1)S(1)}, u32[]{:S(2)}, u32[]{:S(2)}) collective-permute-start(bf16[2,2,32,1024]{3,2,1,0:T(8,128)(2,1)S(1)} %get-tuple-element.16), channel_id=1, source_target_pairs={{64,0},{72,8},{80,16},{88,24},{96,32},{104,40},{112,48},{120,56},{... | collective-permute-start | bytes 786440 | tf_op jit(solution)/shard_map/ppermute | solution.py:16
  116.6 1.9 collective-permute-start.7
  118.6 4.4 %collective-permute-start.13 = (bf16[4,4,32,1024]{3,2,1,0:T(8,128)(2,1)S(1)}, bf16[4,4,32,1024]{3,2,1,0:T(8,128)(2,1)}, u32[]{:S(2)}, u32[]{:S(2)}) collective-permute-start(bf16[4,4,32,1024]{3,2,1,0:T(8,128)(2,1)S(1)} %bitcast_dynamic-update-slice_fusion.8), channel_id=1, source_target_pairs={{16,0},{24,8},{0,16},{8,24},{48,32},{56,40},{32,48},{40,56},{80,64... | collective-permute-start | bytes 3145736 | tf_op jit(solution)/shard_map/ppermute | solution.py:16
  123.0 1.7 broadcast_in_dim.111
  124.7 0.9 bitcast_dynamic-update-slice_fusion.2
  125.5 0.8 bitcast_dynamic-update-slice_fusion.1
  126.5 0.7 bitcast_dynamic-update-slice_fusion.4
  127.2 4.4 %collective-permute-done.7 = bf16[2,2,32,1024]{3,2,1,0:T(8,128)(2,1)S(1)} collective-permute-done((bf16[2,2,32,1024]{3,2,1,0:T(8,128)(2,1)S(1)}, bf16[2,2,32,1024]{3,2,1,0:T(8,128)(2,1)S(1)}, u32[]{:S(2)}, u32[]{:S(2)}) %collective-permute-start.7) | collective-permute-done | bytes 262176 | tf_op jit(solution)/shard_map/ppermute | solution.py:16
  131.6 0.7 bitcast_dynamic-update-slice_fusion.6
  132.3 8.9 %collective-permute-start.8 = (bf16[1024,1024]{1,0:T(8,128)(2,1)}, bf16[1024,1024]{1,0:T(8,128)(2,1)}, u32[]{:S(2)}, u32[]{:S(2)}) collective-permute-start(bf16[1024,1024]{1,0:T(8,128)(2,1)} %bitcast.46), channel_id=1, source_target_pairs={{0,1},{1,0},{2,3},{3,2},{4,5},{5,4},{6,7},{7,6},{8,9},{9,8},{10,11... | collective-permute-start | bytes 6291464 | tf_op jit(solution)/shard_map/ppermute | solution.py:76
  142.0 1.3 broadcast_in_dim.106
  143.4 4.9 %all-to-all-start.1 = ((bf16[8,48,2048]{2,1,0:T(8,128)(2,1)}), bf16[8,48,2048]{2,1,0:T(8,128)(2,1)}, u32[]{:S(2)}, u32[]{:S(2)}) async-start(bf16[8,48,2048]{2,1,0:T(8,128)(2,1)} %broadcast_in_dim.106), calls=%async_computation.1 | async-start | bytes 3145728 | tf_op jit(solution)/shard_map/all_to_all | solution.py:89
  148.2 1.6 broadcast_in_dim.122
  149.9 2.3 %bitcast_dynamic-update-slice_fusion = bf16[4,4,2,32,1024]{4,3,2,1,0:T(8,128)(2,1)} fusion(bf16[4,4,2,32,1024]{4,3,2,1,0:T(8,128)(2,1)} %broadcast_in_dim.122, s32[]{:T(128)S(6)} %select_n.144, bf16[4,4,32,1024]{3,2,1,0:T(8,128)(2,1)} %collective-permute-done.13), kind=kLoop, calls=%fused_computation.15 | loop fusion | bytes 2097156 | tf_op jit(solution)/shard_map/dynamic_update_slice | solution.py:60
  152.2 2.2 %collective-permute-start.14 = (bf16[1024,1024]{1,0:T(8,128)(2,1)}, bf16[1024,1024]{1,0:T(8,128)(2,1)}, u32[]{:S(2)}, u32[]{:S(2)}) collective-permute-start(bf16[1024,1024]{1,0:T(8,128)(2,1)} %bitcast.56), channel_id=1, source_target_pairs={{0,1},{1,0},{2,3},{3,2},{4,5},{5,4},{6,7},{7,6},{8,9},{9,8},{10,11... | collective-permute-start | bytes 6291464 | tf_op jit(solution)/shard_map/ppermute | solution.py:76
  154.4 15.5 %all-to-all-done.1 = bf16[8,48,2048]{2,1,0:T(8,128)(2,1)} async-done(((bf16[8,48,2048]{2,1,0:T(8,128)(2,1)}), bf16[8,48,2048]{2,1,0:T(8,128)(2,1)}, u32[]{:S(2)}, u32[]{:S(2)}) %all-to-all-start.1) | async-done | bytes 1572896 | tf_op jit(solution)/shard_map/all_to_all | solution.py:89
  169.8 2.8 %fusion.4 = f32[384,1024]{1,0:T(8,128)S(1)} fusion(bf16[1024,1024]{1,0:T(8,128)(2,1)} %collective-permute-done.8, bf16[384,2048]{1,0:T(8,128)(2,1)} %bitcast.33), kind=kOutput, calls=%fused_computation.18 | convolution fusion | flops 805306368 | bytes 4456448 | tf_op jit(solution)/shard_map/dot_general | solution.py:224
  172.6 2.8 %multiply_convert_fusion = bf16[384,1024]{1,0:T(8,128)(2,1)S(1)} fusion(f32[384,1024]{1,0:T(8,128)S(1)} %fusion.4, bf16[1024,1024]{1,0:T(8,128)(2,1)} %bitcast.46, bf16[384,2048]{1,0:T(8,128)(2,1)} %bitcast.33), kind=kOutput, calls=%fused_computation.4 | convolution fusion | flops 806879232 | bytes 5242880 | tf_op jit(solution)/shard_map/dot_general | solution.py:224
  175.5 2.6 %convolution_convert_fusion.2 = bf16[384,1024]{1,0:T(8,128)(2,1)S(1)} fusion(bf16[384,1024]{1,0:T(8,128)(2,1)S(1)} %multiply_convert_fusion, bf16[1024,1024]{1,0:T(8,128)(2,1)} %bitcast.56), kind=kOutput, calls=%fused_computation.8 | convolution fusion | flops 805699584 | bytes 3670016 | tf_op jit(solution)/shard_map/dot_general | solution.py:230
  178.1 2.6 %convolution_convert_fusion.1 = bf16[384,1024]{1,0:T(8,128)(2,1)S(1)} fusion(bf16[384,1024]{1,0:T(8,128)(2,1)S(1)} %multiply_convert_fusion, bf16[1024,1024]{1,0:T(8,128)(2,1)} %collective-permute-done.14), kind=kOutput, calls=%fused_computation.7 | convolution fusion | flops 805699584 | bytes 3670016 | tf_op jit(solution)/shard_map/dot_general | solution.py:230
  180.9 24.5 %all_to_all.20 = bf16[8,48,2048]{2,1,0:T(8,128)(2,1)S(1)} all-to-all(bf16[8,48,2048]{2,1,0:T(8,128)(2,1)S(1)} %bitcast.138), channel_id=1, replica_groups={{0,2,4,6,8,10,12,14},{1,3,5,7,9,11,13,15},{16,18,20,22,24,26,28,30},{17..., dimensions={0} | all-to-all | bytes 3145728 | tf_op jit(solution)/shard_map/all_to_all | solution.py:89
  207.2 0.8 fusion.13
  (79 shorter events, 5.6 us)
Async XLA Ops:
  0.0 14.4 %copy-start = (bf16[256,2048]{1,0:T(8,128)(2,1)S(1)}, bf16[256,2048]{1,0:T(8,128)(2,1)}, u32[]{:S(2)}) copy-start(bf16[256,2048]{1,0:T(8,128)(2,1)} %param.18) | copy-start | bytes 3145732
  1.9 10.3 %copy-start.1 = (bf16[384,128]{1,0:T(8,128)(2,1)S(1)}, bf16[384,128]{1,0:T(8,128)(2,1)}, u32[]{:S(2)}) copy-start(bf16[384,128]{1,0:T(8,128)(2,1)} %param.14) | copy-start | bytes 294916
  2.8 9.5 %collective-permute-start = (bf16[2,128,128]{2,1,0:T(8,128)(2,1)S(1)}, bf16[2,128,128]{2,1,0:T(8,128)(2,1)S(1)}, u32[]{:S(2)}, u32[]{:S(2)}) collective-permute-start(bf16[2,128,128]{2,1,0:T(8,128)(2,1)S(1)} %get-tuple-element.25), channel_id=1, source_target_pairs={{0,8},{8,16},{16,24},{24,32},{32,40},{40,48},{48,56},{56,64},{64,7... | collective-permute-start | bytes 196616 | tf_op jit(solution)/shard_map/ppermute | solution.py:122
  6.9 5.4 %collective-permute-start.1 = (bf16[2,128,128]{2,1,0:T(8,128)(2,1)S(1)}, bf16[2,128,128]{2,1,0:T(8,128)(2,1)S(1)}, u32[]{:S(2)}, u32[]{:S(2)}) collective-permute-start(bf16[2,128,128]{2,1,0:T(8,128)(2,1)S(1)} %get-tuple-element.26), channel_id=1, source_target_pairs={{8,0},{16,8},{24,16},{32,24},{40,32},{48,40},{56,48},{64,56},{72,6... | collective-permute-start | bytes 196616 | tf_op jit(solution)/shard_map/ppermute | solution.py:123
  12.4 0.7 copy-start.7
  16.1 8.4 %copy-start.2 = (bf16[1024,32]{0,1:T(8,128)(2,1)S(1)}, bf16[1024,32]{0,1:T(8,128)(2,1)}, u32[]{:S(2)}) copy-start(bf16[1024,32]{0,1:T(8,128)(2,1)} %param.21) | copy-start | bytes 196612
  16.1 8.4 %copy-start.3 = (bf16[32,1024]{1,0:T(8,128)(2,1)S(1)}, bf16[32,1024]{1,0:T(8,128)(2,1)}, u32[]{:S(2)}) copy-start(bf16[32,1024]{1,0:T(8,128)(2,1)} %param.20) | copy-start | bytes 196612
  16.1 29.0 %all-to-all-start = ((bf16[8,48,2048]{2,1,0:T(8,128)(2,1)}), bf16[8,48,2048]{2,1,0:T(8,128)(2,1)S(1)}, u32[]{:S(2)}, u32[]{:S(2)}) async-start(bf16[8,48,2048]{2,1,0:T(8,128)(2,1)} %bitcast.139), calls=%async_computation | async-start | bytes 3145728 | tf_op jit(solution)/shard_map/all_to_all | solution.py:135
  24.6 6.6 %collective-permute-start.2 = (bf16[2,32,1024]{2,1,0:T(8,128)(2,1)S(1)}, bf16[2,32,1024]{2,1,0:T(8,128)(2,1)S(1)}, u32[]{:S(2)}, u32[]{:S(2)}) collective-permute-start(bf16[2,32,1024]{2,1,0:T(8,128)(2,1)S(1)} %pad_maximum_fusion.3), channel_id=1, source_target_pairs={{0,0},{1,8},{2,2},{3,10},{4,4},{5,12},{6,6},{7,14},{8,1},{9,9},{10... | collective-permute-start | bytes 393224 | tf_op jit(solution)/shard_map/ppermute | solution.py:72
  46.0 16.6 %copy-start.4 = (f32[2048]{0:T(1024)S(1)}, f32[2048]{0:T(1024)}, u32[]{:S(2)}) copy-start(f32[2048]{0:T(1024)} %param.19) | copy-start | bytes 24580
  46.1 44.5 %all-to-all-start.2 = ((bf16[4,2,32,1024]{3,2,1,0:T(8,128)(2,1)}), bf16[4,2,32,1024]{3,2,1,0:T(8,128)(2,1)S(1)}, u32[]{:S(2)}, u32[]{:S(2)}) async-start(bf16[4,2,32,1024]{3,2,1,0:T(8,128)(2,1)} %broadcast_in_dim.107), calls=%async_computation.2 | async-start | bytes 1048576 | tf_op jit(solution)/shard_map/all_to_all | solution.py:34
  90.6 14.9 %collective-permute-start.3 = (bf16[4,32,1024]{2,1,0:T(8,128)(2,1)S(1)}, bf16[4,32,1024]{2,1,0:T(8,128)(2,1)S(1)}, u32[]{:S(2)}, u32[]{:S(2)}) collective-permute-start(bf16[4,32,1024]{2,1,0:T(8,128)(2,1)S(1)} %get-tuple-element.12), channel_id=1, source_target_pairs={{16,0},{24,8},{0,16},{8,24},{48,32},{56,40},{32,48},{40,56},{80,64... | collective-permute-start | bytes 786440 | tf_op jit(solution)/shard_map/ppermute | solution.py:16
  92.5 17.4 %collective-permute-start.9 = (bf16[4,32,1024]{2,1,0:T(8,128)(2,1)S(1)}, bf16[4,32,1024]{2,1,0:T(8,128)(2,1)S(1)}, u32[]{:S(2)}, u32[]{:S(2)}) collective-permute-start(bf16[4,32,1024]{2,1,0:T(8,128)(2,1)S(1)} %get-tuple-element.11), channel_id=1, source_target_pairs={{32,0},{40,8},{48,16},{56,24},{64,32},{72,40},{80,48},{88,56},{96,... | collective-permute-start | bytes 786440 | tf_op jit(solution)/shard_map/ppermute | solution.py:16
  95.6 16.4 %collective-permute-start.10 = (bf16[4,32,1024]{2,1,0:T(8,128)(2,1)S(1)}, bf16[4,32,1024]{2,1,0:T(8,128)(2,1)S(1)}, u32[]{:S(2)}, u32[]{:S(2)}) collective-permute-start(bf16[4,32,1024]{2,1,0:T(8,128)(2,1)S(1)} %get-tuple-element.11), channel_id=1, source_target_pairs={{480,0},{488,8},{496,16},{504,24},{0,32},{8,40},{16,48},{24,56},{3... | collective-permute-start | bytes 786440 | tf_op jit(solution)/shard_map/ppermute | solution.py:16
  98.1 18.6 %collective-permute-start.11 = (bf16[2,32,1024]{2,1,0:T(8,128)(2,1)S(1)}, bf16[2,32,1024]{2,1,0:T(8,128)(2,1)S(1)}, u32[]{:S(2)}, u32[]{:S(2)}) collective-permute-start(bf16[2,32,1024]{2,1,0:T(8,128)(2,1)S(1)} %get-tuple-element.10), channel_id=1, source_target_pairs={{64,0},{72,8},{80,16},{88,24},{96,32},{104,40},{112,48},{120,56},{... | collective-permute-start | bytes 393224 | tf_op jit(solution)/shard_map/ppermute | solution.py:16
  103.6 15.0 %collective-permute-start.12 = (bf16[2,32,1024]{2,1,0:T(8,128)(2,1)S(1)}, bf16[2,32,1024]{2,1,0:T(8,128)(2,1)S(1)}, u32[]{:S(2)}, u32[]{:S(2)}) collective-permute-start(bf16[2,32,1024]{2,1,0:T(8,128)(2,1)S(1)} %get-tuple-element.9), channel_id=1, source_target_pairs={{448,0},{456,8},{464,16},{472,24},{480,32},{488,40},{496,48},{504,... | collective-permute-start | bytes 393224 | tf_op jit(solution)/shard_map/ppermute | solution.py:16
  105.6 17.4 %collective-permute-start.4 = (bf16[4,2,32,1024]{3,2,1,0:T(8,128)(2,1)S(1)}, bf16[4,2,32,1024]{3,2,1,0:T(8,128)(2,1)S(1)}, u32[]{:S(2)}, u32[]{:S(2)}) collective-permute-start(bf16[4,2,32,1024]{3,2,1,0:T(8,128)(2,1)S(1)} %bitcast_dynamic-update-slice_fusion.7), channel_id=1, source_target_pairs={{32,0},{40,8},{48,16},{56,24},{64,32},{72,40},{80,48},{88,56},{96,... | collective-permute-start | bytes 1572872 | tf_op jit(solution)/shard_map/ppermute | solution.py:16
  109.9 15.6 %collective-permute-start.5 = (bf16[4,2,32,1024]{3,2,1,0:T(8,128)(2,1)S(1)}, bf16[4,2,32,1024]{3,2,1,0:T(8,128)(2,1)S(1)}, u32[]{:S(2)}, u32[]{:S(2)}) collective-permute-start(bf16[4,2,32,1024]{3,2,1,0:T(8,128)(2,1)S(1)} %bitcast_dynamic-update-slice_fusion.7), channel_id=1, source_target_pairs={{480,0},{488,8},{496,16},{504,24},{0,32},{8,40},{16,48},{24,56},{3... | collective-permute-start | bytes 1572872 | tf_op jit(solution)/shard_map/ppermute | solution.py:16
  112.1 14.4 %collective-permute-start.6 = (bf16[2,2,32,1024]{3,2,1,0:T(8,128)(2,1)S(1)}, bf16[2,2,32,1024]{3,2,1,0:T(8,128)(2,1)S(1)}, u32[]{:S(2)}, u32[]{:S(2)}) collective-permute-start(bf16[2,2,32,1024]{3,2,1,0:T(8,128)(2,1)S(1)} %get-tuple-element.16), channel_id=1, source_target_pairs={{64,0},{72,8},{80,16},{88,24},{96,32},{104,40},{112,48},{120,56},{... | collective-permute-start | bytes 786440 | tf_op jit(solution)/shard_map/ppermute | solution.py:16
  116.6 15.0 %collective-permute-start.7 = (bf16[2,2,32,1024]{3,2,1,0:T(8,128)(2,1)S(1)}, bf16[2,2,32,1024]{3,2,1,0:T(8,128)(2,1)S(1)}, u32[]{:S(2)}, u32[]{:S(2)}) collective-permute-start(bf16[2,2,32,1024]{3,2,1,0:T(8,128)(2,1)S(1)} %get-tuple-element.15), channel_id=1, source_target_pairs={{448,0},{456,8},{464,16},{472,24},{480,32},{488,40},{496,48},{504,... | collective-permute-start | bytes 786440 | tf_op jit(solution)/shard_map/ppermute | solution.py:16
  118.6 29.6 %collective-permute-start.13 = (bf16[4,4,32,1024]{3,2,1,0:T(8,128)(2,1)S(1)}, bf16[4,4,32,1024]{3,2,1,0:T(8,128)(2,1)}, u32[]{:S(2)}, u32[]{:S(2)}) collective-permute-start(bf16[4,4,32,1024]{3,2,1,0:T(8,128)(2,1)S(1)} %bitcast_dynamic-update-slice_fusion.8), channel_id=1, source_target_pairs={{16,0},{24,8},{0,16},{8,24},{48,32},{56,40},{32,48},{40,56},{80,64... | collective-permute-start | bytes 3145736 | tf_op jit(solution)/shard_map/ppermute | solution.py:16
  124.7 16.6 %copy-start.6 = (f32[2048]{0:T(1024)S(1)}, f32[2048]{0:T(1024)}, u32[]{:S(2)}) copy-start(f32[2048]{0:T(1024)} %param.22) | copy-start | bytes 24580
  132.3 37.5 %collective-permute-start.8 = (bf16[1024,1024]{1,0:T(8,128)(2,1)}, bf16[1024,1024]{1,0:T(8,128)(2,1)}, u32[]{:S(2)}, u32[]{:S(2)}) collective-permute-start(bf16[1024,1024]{1,0:T(8,128)(2,1)} %bitcast.46), channel_id=1, source_target_pairs={{0,1},{1,0},{2,3},{3,2},{4,5},{5,4},{6,7},{7,6},{8,9},{9,8},{10,11... | collective-permute-start | bytes 6291464 | tf_op jit(solution)/shard_map/ppermute | solution.py:76
  143.4 26.5 %all-to-all-start.1 = ((bf16[8,48,2048]{2,1,0:T(8,128)(2,1)}), bf16[8,48,2048]{2,1,0:T(8,128)(2,1)}, u32[]{:S(2)}, u32[]{:S(2)}) async-start(bf16[8,48,2048]{2,1,0:T(8,128)(2,1)} %broadcast_in_dim.106), calls=%async_computation.1 | async-start | bytes 3145728 | tf_op jit(solution)/shard_map/all_to_all | solution.py:89
  152.2 25.9 %collective-permute-start.14 = (bf16[1024,1024]{1,0:T(8,128)(2,1)}, bf16[1024,1024]{1,0:T(8,128)(2,1)}, u32[]{:S(2)}, u32[]{:S(2)}) collective-permute-start(bf16[1024,1024]{1,0:T(8,128)(2,1)} %bitcast.56), channel_id=1, source_target_pairs={{0,1},{1,0},{2,3},{3,2},{4,5},{5,4},{6,7},{7,6},{8,9},{9,8},{10,11... | collective-permute-start | bytes 6291464 | tf_op jit(solution)/shard_map/ppermute | solution.py:76
  206.5 0.7 copy-start.5

commit v2 on v1

--- a/solution.py
+++ b/solution.py
@@ -45,13 +45,6 @@
     return fetch(shard[:half], 2, 0), fetch(shard[half:], -2, 0)
 
 
-def joined_z(shard, near, far, dim, own_at):
-    half = shard.shape[0] // 2
-    pieces = [(near[0], 1, 0, 0), (near[1], 3, 0, 0)]
-    pieces += [(far[0], 2, 0, 0), (far[1], 2, 0, half)]
-    return placed(shard, pieces, dim, own_at)
-
-
 def joined_y(shard, other, dim, own_at):
     whole = jnp.expand_dims(shard, dim)
     whole = jnp.broadcast_to(whole, (*whole.shape[:dim], 2, *whole.shape[dim + 1 :]))
@@ -101,14 +94,19 @@
     z, y = (place // 4, place % 4)
     both = paired(jnp.stack([up_proj, down_proj.T]))
     far = far_stage(both)
-    up, down = (far[:, 0], far[:, 1])
-    up_other = fetch(up, 0, 2)
-    down_near, down_far = (beside(down, "z"), across_z(down))
-    up = joined_y(up, up_other, 1, y // 2)
-    down = joined_z(down, down_near, down_far, 1, z % 4)
-    up_near, up_far, down_other = (beside(up, "z"), across_z(up), fetch(down, 0, 2))
-    up = joined_z(up, up_near, up_far, 1, z % 4).reshape(1024, 1024)
-    down = joined_y(down, down_other, 2, y // 2).reshape(1024, 1024)
+    both = far.swapaxes(0, 1)
+    other = fetch(both, 0, 2)
+    both = joined_y(both, other, 2, y // 2)
+    near, across = (beside(both, "z"), across_z(both))
+    up, down = (
+        placed(
+            both[i],
+            [(near[0][i], 1, 0, 0), (near[1][i], 3, 0, 0), (across[i][0], 2, 0, 0)],
+            1,
+            z % 4,
+        ).reshape(1024, 1024)
+        for i in range(2)
+    )
     return up, swapped(up), down, swapped(down)
 
 

time: 211 us -> 221 us (1.047)
  waiting for transfers between devices: 63.7 us -> 97.5 us
  starting transfers between devices: 81.4 us -> 59.4 us
  other arithmetic: 7.53 us -> 10.3 us
    ppermute x10 -> x5, waiting for transfers between devices: 4.55 us -> 48.8 us  [fetch(): return lax.ppermute(shard, 'sp', pairs)]
    ppermute x10 -> x5, starting transfers between devices: 31.8 us -> 16.1 us  [fetch(): return lax.ppermute(shard, 'sp', pairs)]
    all_to_all x1, waiting for transfers between devices: 15.5 us -> 3.88 us  [exchanged(): lax.all_to_all(pieces, ('sp', 'tp'), 0, 0, axis_index_groups=token_groups...]
    all_to_all x1, starting transfers between devices: 16.3 us -> 20.8 us  [far_stage(): lax.all_to_all(spread, 'sp', 0, 0, axis_index_groups=groups, tiled=True)]
    ppermute x2, starting transfers between devices: 11.1 us -> 6.56 us  [swapped(): return lax.ppermute(shard, 'tp', [(i, i ^ 1) for i in range(8)])]
    all_to_all x1, starting transfers between devices: 8.43 us -> 4.41 us  [summed_on_arrival(): lax.all_to_all(pieces, axis, split_axis=0, concat_axis=0, tiled=True)]
    all_to_all x1, waiting for transfers between devices: 14 us -> 17.4 us  [summed_on_arrival(): lax.all_to_all(pieces, axis, split_axis=0, concat_axis=0, tiled=True)]
    ppermute x1, waiting for transfers between devices: 3 us -> 0.01 us  [paired(): return lax.ppermute(shard, ('sp', 'tp'), pairs)]
  transfers between devices with their start and end apart: 18 -> 13, of which waited for: 6 -> 7; matrix products, arithmetic and copies ran while one was open for 12% -> 13% of each run, Pallas kernels for 0% -> 0%
where the time goes in v2:
time: 221 us; the launch traced here: 220 us
  waiting for transfers between devices  97.5 us (44%)
  starting transfers between devices  59.4 us (27%)
  blocking collectives  24.5 us (11%)
  local copies, waits for them, and re-layouts  16 us (7%)
  matrix products  11.3 us (5%)
  other arithmetic  10.3 us (5%)
    ppermute x5, waiting for transfers between devices, fetch(): return lax.ppermute(shard, 'sp', pairs)  48.8 us
    all_to_all x1, waiting for transfers between devices, far_stage(): lax.all_to_all(spread, 'sp', 0, 0, axis_index_groups=groups, tiled=True)  27.4 us
    all_to_all x1, blocking collectives, exchanged(): lax.all_to_all(pieces, ('sp', 'tp'), 0, 0, axis_index_groups=token_groups...  24.5 us
    all_to_all x1, starting transfers between devices, far_stage(): lax.all_to_all(spread, 'sp', 0, 0, axis_index_groups=groups, tiled=True)  20.8 us
    all_to_all x1, waiting for transfers between devices, summed_on_arrival(): lax.all_to_all(pieces, axis, split_axis=0, concat_axis=0, tiled=True)  17.4 us
    ppermute x5, starting transfers between devices, fetch(): return lax.ppermute(shard, 'sp', pairs)  16.1 us
    ppermute x2, starting transfers between devices, swapped(): return lax.ppermute(shard, 'tp', [(i, i ^ 1) for i in range(8)])  6.56 us
    ppermute x1, starting transfers between devices, paired(): return lax.ppermute(shard, ('sp', 'tp'), pairs)  4.58 us
  transfers between devices with their start and end apart: 13, of which 7 were waited for; matrix products, arithmetic and copies ran while one was open for 13% of the time, Pallas kernels for 0%

profile of v2, /device:TPU:1, one launch (start us, length us, event | category | flops | bytes accessed | tf_op | source)
XLA Modules:
  0.0 219.7 jit_solution(18413490991935544588)
XLA Ops:
  0.0 1.0 pad_maximum_fusion.3
  1.0 4.6 %collective-permute-start.2 = (bf16[2,32,1024]{2,1,0:T(8,128)(2,1)S(1)}, bf16[2,32,1024]{2,1,0:T(8,128)(2,1)S(1)}, u32[]{:S(2)}, u32[]{:S(2)}) collective-permute-start(bf16[2,32,1024]{2,1,0:T(8,128)(2,1)S(1)} %pad_maximum_fusion.3), channel_id=1, source_target_pairs={{0,0},{1,8},{2,2},{3,10},{4,4},{5,12},{6,6},{7,14},{8,1},{9,9},{10... | collective-permute-start | bytes 393224 | tf_op jit(solution)/shard_map/ppermute | solution.py:65
  5.6 1.8 fusion.37
  7.5 0.9 pad_maximum_fusion.14
  8.4 1.3 collective-permute-start
  9.7 1.3 collective-permute-start.1
  11.0 0.4 multiply_cosine_fusion.1
  11.4 0.8 pad_dynamic-slice_fusion
  12.2 0.8 dynamic-slice_bitcast_fusion
  14.2 0.9 broadcast_in_dim.38
  15.1 20.8 %all-to-all-start.2 = ((bf16[4,2,32,1024]{3,2,1,0:T(8,128)(2,1)}), bf16[4,2,32,1024]{3,2,1,0:T(8,128)(2,1)S(1)}, u32[]{:S(2)}, u32[]{:S(2)}) async-start(bf16[4,2,32,1024]{3,2,1,0:T(8,128)(2,1)} %broadcast_in_dim.38), calls=%async_computation.2 | async-start | bytes 1048576 | tf_op jit(solution)/shard_map/all_to_all | solution.py:34
  36.3 0.4 fusion.49
  37.2 0.4 fusion.2
  37.8 1.8 convolution_convert_fusion
  39.5 27.4 %all-to-all-done.2 = bf16[4,2,32,1024]{3,2,1,0:T(8,128)(2,1)S(1)} async-done(((bf16[4,2,32,1024]{3,2,1,0:T(8,128)(2,1)}), bf16[4,2,32,1024]{3,2,1,0:T(8,128)(2,1)S(1)}, u32[]{:S(2)}, u32[]{:S(2)}) %all-to-all-start.2) | async-done | bytes 524320 | tf_op jit(solution)/shard_map/all_to_all | solution.py:34
  66.9 0.8 copy-done.3
  67.7 4.4 %all-to-all-start = ((bf16[8,48,2048]{2,1,0:T(8,128)(2,1)}), bf16[8,48,2048]{2,1,0:T(8,128)(2,1)S(1)}, u32[]{:S(2)}, u32[]{:S(2)}) async-start(bf16[8,48,2048]{2,1,0:T(8,128)(2,1)} %bitcast.26), calls=%async_computation | async-start | bytes 3145728 | tf_op jit(solution)/shard_map/all_to_all | solution.py:133
  72.1 1.1 copy.78
  73.2 1.9 collective-permute-start.3
  75.3 17.4 %all-to-all-done = bf16[8,48,2048]{2,1,0:T(8,128)(2,1)S(1)} async-done(((bf16[8,48,2048]{2,1,0:T(8,128)(2,1)}), bf16[8,48,2048]{2,1,0:T(8,128)(2,1)S(1)}, u32[]{:S(2)}, u32[]{:S(2)}) %all-to-all-start) | async-done | bytes 1572896 | tf_op jit(solution)/shard_map/all_to_all | solution.py:133
  93.1 1.1 bitcast_dynamic-update-slice_fusion.2
  94.2 1.9 collective-permute-start.4
  96.2 3.4 %collective-permute-start.5 = (bf16[2,4,2,32,1024]{4,3,2,1,0:T(8,128)(2,1)S(1)}, bf16[2,4,2,32,1024]{4,3,2,1,0:T(8,128)(2,1)S(1)}, u32[]{:S(2)}, u32[]{:S(2)}) collective-permute-start(bf16[2,4,2,32,1024]{4,3,2,1,0:T(8,128)(2,1)S(1)} %bitcast_dynamic-update-slice_fusion.2), channel_id=1, source_target_pairs={{480,0},{488,8},{496,16},{504,24},{0,32},{8,40},{16,48},{24,56},{3... | collective-permute-start | bytes 3145736 | tf_op jit(solution)/shard_map/ppermute | solution.py:16
  99.6 1.2 fusion.14
  100.8 1.0 fusion.48
  101.9 2.2 %collective-permute-start.6 = (bf16[1,4,2,32,1024]{4,3,2,1,0:T(8,128)(2,1)S(1)}, bf16[1,4,2,32,1024]{4,3,2,1,0:T(8,128)(2,1)S(1)}, u32[]{:S(2)}, u32[]{:S(2)}) collective-permute-start(bf16[1,4,2,32,1024]{4,3,2,1,0:T(8,128)(2,1)S(1)} %get-tuple-element.12), channel_id=1, source_target_pairs={{64,0},{72,8},{80,16},{88,24},{96,32},{104,40},{112,48},{120,56},{... | collective-permute-start | bytes 1572872 | tf_op jit(solution)/shard_map/ppermute | solution.py:16
  104.1 17.1 %collective-permute-done.4 = bf16[2,4,2,32,1024]{4,3,2,1,0:T(8,128)(2,1)S(1)} collective-permute-done((bf16[2,4,2,32,1024]{4,3,2,1,0:T(8,128)(2,1)S(1)}, bf16[2,4,2,32,1024]{4,3,2,1,0:T(8,128)(2,1)S(1)}, u32[]{:S(2)}, u32[]{:S(2)}) %collective-permute-start.4) | collective-permute-done | bytes 1048608 | tf_op jit(solution)/shard_map/ppermute | solution.py:16
  121.9 1.2 collective-permute-done.5
  123.2 17.5 %collective-permute-done.6 = bf16[1,4,2,32,1024]{4,3,2,1,0:T(8,128)(2,1)S(1)} collective-permute-done((bf16[1,4,2,32,1024]{4,3,2,1,0:T(8,128)(2,1)S(1)}, bf16[1,4,2,32,1024]{4,3,2,1,0:T(8,128)(2,1)S(1)}, u32[]{:S(2)}, u32[]{:S(2)}) %collective-permute-start.6) | collective-permute-done | bytes 524320 | tf_op jit(solution)/shard_map/ppermute | solution.py:16
  140.7 3.8 %collective-permute-start.7 = (bf16[1024,1024]{1,0:T(8,128)(2,1)S(1)}, bf16[1024,1024]{1,0:T(8,128)(2,1)}, u32[]{:S(2)}, u32[]{:S(2)}) collective-permute-start(bf16[1024,1024]{1,0:T(8,128)(2,1)S(1)} %bitcast.135), channel_id=1, source_target_pairs={{0,1},{1,0},{2,3},{3,2},{4,5},{5,4},{6,7},{7,6},{8,9},{9,8},{10,11... | collective-permute-start | bytes 6291464 | tf_op jit(solution)/shard_map/ppermute | solution.py:69
  144.7 1.0 copy.49
  145.7 6.7 %collective-permute-start.8 = (bf16[1,4,2,32,1024]{4,3,2,1,0:T(8,128)(2,1)}, bf16[1,4,2,32,1024]{4,3,2,1,0:T(8,128)(2,1)}, u32[]{:S(2)}, u32[]{:S(2)}) collective-permute-start(bf16[1,4,2,32,1024]{4,3,2,1,0:T(8,128)(2,1)} %get-tuple-element.9), channel_id=1, source_target_pairs={{448,0},{456,8},{464,16},{472,24},{480,32},{488,40},{496,48},{504,... | collective-permute-start | bytes 1572872 | tf_op jit(solution)/shard_map/ppermute | solution.py:16
  152.4 1.9 broadcast_select_fusion.1
  154.3 1.1 copy.68
  155.4 1.1 copy.69
  156.5 1.4 broadcast_in_dim.37
  157.9 4.3 %all-to-all-start.1 = ((bf16[8,48,2048]{2,1,0:T(8,128)(2,1)}), bf16[8,48,2048]{2,1,0:T(8,128)(2,1)}, u32[]{:S(2)}, u32[]{:S(2)}) async-start(bf16[8,48,2048]{2,1,0:T(8,128)(2,1)} %broadcast_in_dim.37), calls=%async_computation.1 | async-start | bytes 3145728 | tf_op jit(solution)/shard_map/all_to_all | solution.py:82
  162.2 13.0 %collective-permute-done.8 = bf16[1,4,2,32,1024]{4,3,2,1,0:T(8,128)(2,1)} collective-permute-done((bf16[1,4,2,32,1024]{4,3,2,1,0:T(8,128)(2,1)}, bf16[1,4,2,32,1024]{4,3,2,1,0:T(8,128)(2,1)}, u32[]{:S(2)}, u32[]{:S(2)}) %collective-permute-start.8) | collective-permute-done | bytes 524320 | tf_op jit(solution)/shard_map/ppermute | solution.py:16
  175.1 1.9 bitcast_dynamic-update-slice_fusion
  177.0 2.8 %collective-permute-start.9 = (bf16[1024,1024]{1,0:T(8,128)(2,1)}, bf16[1024,1024]{1,0:T(8,128)(2,1)}, u32[]{:S(2)}, u32[]{:S(2)}) collective-permute-start(bf16[1024,1024]{1,0:T(8,128)(2,1)} %bitcast.137), channel_id=1, source_target_pairs={{0,1},{1,0},{2,3},{3,2},{4,5},{5,4},{6,7},{7,6},{8,9},{9,8},{10,11... | collective-permute-start | bytes 6291464 | tf_op jit(solution)/shard_map/ppermute | solution.py:69
  179.8 3.9 %all-to-all-done.1 = bf16[8,48,2048]{2,1,0:T(8,128)(2,1)} async-done(((bf16[8,48,2048]{2,1,0:T(8,128)(2,1)}), bf16[8,48,2048]{2,1,0:T(8,128)(2,1)}, u32[]{:S(2)}, u32[]{:S(2)}) %all-to-all-start.1) | async-done | bytes 1572896 | tf_op jit(solution)/shard_map/all_to_all | solution.py:82
  183.7 2.8 %fusion.4 = f32[384,1024]{1,0:T(8,128)S(1)} fusion(bf16[1024,1024]{1,0:T(8,128)(2,1)} %collective-permute-done.7, bf16[384,2048]{1,0:T(8,128)(2,1)} %bitcast.33), kind=kOutput, calls=%fused_computation.17 | convolution fusion | flops 805306368 | bytes 4456448 | tf_op jit(solution)/shard_map/dot_general | solution.py:222
  186.5 2.3 %multiply_convert_fusion = bf16[384,1024]{1,0:T(8,128)(2,1)S(1)} fusion(f32[384,1024]{1,0:T(8,128)S(1)} %fusion.4, bf16[1024,1024]{1,0:T(8,128)(2,1)S(1)} %bitcast.136, bf16[384,2048]{1,0:T(8,128)(2,1)} %bitcast.33), kind=kOutput, calls=%fused_computation.4 | convolution fusion | flops 806879232 | bytes 5242880 | tf_op jit(solution)/shard_map/dot_general | solution.py:222
  188.8 1.0 convolution_convert_fusion.2
  189.9 2.6 %convolution_convert_fusion.1 = bf16[384,1024]{1,0:T(8,128)(2,1)S(1)} fusion(bf16[384,1024]{1,0:T(8,128)(2,1)S(1)} %multiply_convert_fusion, bf16[1024,1024]{1,0:T(8,128)(2,1)} %collective-permute-done.9), kind=kOutput, calls=%fused_computation.7 | convolution fusion | flops 805699584 | bytes 3670016 | tf_op jit(solution)/shard_map/dot_general | solution.py:228
  192.6 24.5 %all_to_all.20 = bf16[8,48,2048]{2,1,0:T(8,128)(2,1)S(1)} all-to-all(bf16[8,48,2048]{2,1,0:T(8,128)(2,1)S(1)} %bitcast.133), channel_id=1, replica_groups={{0,2,4,6,8,10,12,14},{1,3,5,7,9,11,13,15},{16,18,20,22,24,26,28,30},{17..., dimensions={0} | all-to-all | bytes 3145728 | tf_op jit(solution)/shard_map/all_to_all | solution.py:82
  217.4 0.3 copy.71
  218.9 0.8 fusion.17
  (66 shorter events, 5.0 us)
Async XLA Ops:
  0.0 37.8 %copy-start = (bf16[256,2048]{1,0:T(8,128)(2,1)S(1)}, bf16[256,2048]{1,0:T(8,128)(2,1)}, u32[]{:S(2)}) copy-start(bf16[256,2048]{1,0:T(8,128)(2,1)} %param.18) | copy-start | bytes 3145732
  0.0 13.1 %copy-start.5 = (bf16[384,256]{1,0:T(8,128)(2,1)S(1)}, bf16[384,256]{1,0:T(8,128)(2,1)}, u32[]{:S(2)}) copy-start(bf16[384,256]{1,0:T(8,128)(2,1)} %param.12) | copy-start | bytes 589828
  1.0 13.2 %collective-permute-start.2 = (bf16[2,32,1024]{2,1,0:T(8,128)(2,1)S(1)}, bf16[2,32,1024]{2,1,0:T(8,128)(2,1)S(1)}, u32[]{:S(2)}, u32[]{:S(2)}) collective-permute-start(bf16[2,32,1024]{2,1,0:T(8,128)(2,1)S(1)} %pad_maximum_fusion.3), channel_id=1, source_target_pairs={{0,0},{1,8},{2,2},{3,10},{4,4},{5,12},{6,6},{7,14},{8,1},{9,9},{10... | collective-permute-start | bytes 393224 | tf_op jit(solution)/shard_map/ppermute | solution.py:65
  7.4 6.6 %copy-start.4 = (bf16[384,128]{1,0:T(8,128)(2,1)S(1)}, bf16[384,128]{1,0:T(8,128)(2,1)}, u32[]{:S(2)}) copy-start(bf16[384,128]{1,0:T(8,128)(2,1)} %param.14) | copy-start | bytes 294916
  8.4 27.5 %collective-permute-start = (bf16[2,128,128]{2,1,0:T(8,128)(2,1)S(1)}, bf16[2,128,128]{2,1,0:T(8,128)(2,1)S(1)}, u32[]{:S(2)}, u32[]{:S(2)}) collective-permute-start(bf16[2,128,128]{2,1,0:T(8,128)(2,1)S(1)} %get-tuple-element.27), channel_id=1, source_target_pairs={{0,8},{8,16},{16,24},{24,32},{32,40},{40,48},{48,56},{56,64},{64,7... | collective-permute-start | bytes 196616 | tf_op jit(solution)/shard_map/ppermute | solution.py:120
  9.7 26.2 %collective-permute-start.1 = (bf16[2,128,128]{2,1,0:T(8,128)(2,1)S(1)}, bf16[2,128,128]{2,1,0:T(8,128)(2,1)S(1)}, u32[]{:S(2)}, u32[]{:S(2)}) collective-permute-start(bf16[2,128,128]{2,1,0:T(8,128)(2,1)S(1)} %get-tuple-element.28), channel_id=1, source_target_pairs={{8,0},{16,8},{24,16},{32,24},{40,32},{48,40},{56,48},{64,56},{72,6... | collective-permute-start | bytes 196616 | tf_op jit(solution)/shard_map/ppermute | solution.py:121
  15.1 51.8 %all-to-all-start.2 = ((bf16[4,2,32,1024]{3,2,1,0:T(8,128)(2,1)}), bf16[4,2,32,1024]{3,2,1,0:T(8,128)(2,1)S(1)}, u32[]{:S(2)}, u32[]{:S(2)}) async-start(bf16[4,2,32,1024]{3,2,1,0:T(8,128)(2,1)} %broadcast_in_dim.38), calls=%async_computation.2 | async-start | bytes 1048576 | tf_op jit(solution)/shard_map/all_to_all | solution.py:34
  36.0 0.7 copy-start.9
  66.9 0.8 copy-start.3
  67.7 25.0 %all-to-all-start = ((bf16[8,48,2048]{2,1,0:T(8,128)(2,1)}), bf16[8,48,2048]{2,1,0:T(8,128)(2,1)S(1)}, u32[]{:S(2)}, u32[]{:S(2)}) async-start(bf16[8,48,2048]{2,1,0:T(8,128)(2,1)} %bitcast.26), calls=%async_computation | async-start | bytes 3145728 | tf_op jit(solution)/shard_map/all_to_all | solution.py:133
  73.2 19.7 %collective-permute-start.3 = (bf16[2,4,32,1024]{3,2,1,0:T(8,128)(2,1)S(1)}, bf16[2,4,32,1024]{3,2,1,0:T(8,128)(2,1)}, u32[]{:S(2)}, u32[]{:S(2)}) collective-permute-start(bf16[2,4,32,1024]{3,2,1,0:T(8,128)(2,1)S(1)} %bitcast.139), channel_id=1, source_target_pairs={{16,0},{24,8},{0,16},{8,24},{48,32},{56,40},{32,48},{40,56},{80,64... | collective-permute-start | bytes 1572872 | tf_op jit(solution)/shard_map/ppermute | solution.py:16
  92.9 6.7 %copy-start.6 = (f32[2048]{0:T(1024)S(1)}, f32[2048]{0:T(1024)}, u32[]{:S(2)}) copy-start(f32[2048]{0:T(1024)} %param.19) | copy-start | bytes 24580
  94.2 27.0 %collective-permute-start.4 = (bf16[2,4,2,32,1024]{4,3,2,1,0:T(8,128)(2,1)S(1)}, bf16[2,4,2,32,1024]{4,3,2,1,0:T(8,128)(2,1)S(1)}, u32[]{:S(2)}, u32[]{:S(2)}) collective-permute-start(bf16[2,4,2,32,1024]{4,3,2,1,0:T(8,128)(2,1)S(1)} %bitcast_dynamic-update-slice_fusion.2), channel_id=1, source_target_pairs={{32,0},{40,8},{48,16},{56,24},{64,32},{72,40},{80,48},{88,56},{96,... | collective-permute-start | bytes 3145736 | tf_op jit(solution)/shard_map/ppermute | solution.py:16
  96.2 26.8 %collective-permute-start.5 = (bf16[2,4,2,32,1024]{4,3,2,1,0:T(8,128)(2,1)S(1)}, bf16[2,4,2,32,1024]{4,3,2,1,0:T(8,128)(2,1)S(1)}, u32[]{:S(2)}, u32[]{:S(2)}) collective-permute-start(bf16[2,4,2,32,1024]{4,3,2,1,0:T(8,128)(2,1)S(1)} %bitcast_dynamic-update-slice_fusion.2), channel_id=1, source_target_pairs={{480,0},{488,8},{496,16},{504,24},{0,32},{8,40},{16,48},{24,56},{3... | collective-permute-start | bytes 3145736 | tf_op jit(solution)/shard_map/ppermute | solution.py:16
  101.9 38.8 %collective-permute-start.6 = (bf16[1,4,2,32,1024]{4,3,2,1,0:T(8,128)(2,1)S(1)}, bf16[1,4,2,32,1024]{4,3,2,1,0:T(8,128)(2,1)S(1)}, u32[]{:S(2)}, u32[]{:S(2)}) collective-permute-start(bf16[1,4,2,32,1024]{4,3,2,1,0:T(8,128)(2,1)S(1)} %get-tuple-element.12), channel_id=1, source_target_pairs={{64,0},{72,8},{80,16},{88,24},{96,32},{104,40},{112,48},{120,56},{... | collective-permute-start | bytes 1572872 | tf_op jit(solution)/shard_map/ppermute | solution.py:16
  123.1 21.4 %copy-start.8 = (f32[2048]{0:T(1024)S(1)}, f32[2048]{0:T(1024)}, u32[]{:S(2)}) copy-start(f32[2048]{0:T(1024)} %param.22) | copy-start | bytes 24580
  123.2 17.5 %copy-start.1 = (bf16[4,4,2,32,1024]{4,3,2,1,0:T(8,128)(2,1)}, bf16[4,4,2,32,1024]{4,3,2,1,0:T(8,128)(2,1)S(1)}, u32[]{:S(2)}) copy-start(bf16[4,4,2,32,1024]{4,3,2,1,0:T(8,128)(2,1)S(1)} %get-tuple-element.13) | copy-start | bytes 6291460
  140.7 42.9 %collective-permute-start.7 = (bf16[1024,1024]{1,0:T(8,128)(2,1)S(1)}, bf16[1024,1024]{1,0:T(8,128)(2,1)}, u32[]{:S(2)}, u32[]{:S(2)}) collective-permute-start(bf16[1024,1024]{1,0:T(8,128)(2,1)S(1)} %bitcast.135), channel_id=1, source_target_pairs={{0,1},{1,0},{2,3},{3,2},{4,5},{5,4},{6,7},{7,6},{8,9},{9,8},{10,11... | collective-permute-start | bytes 6291464 | tf_op jit(solution)/shard_map/ppermute | solution.py:69
  145.7 29.4 %collective-permute-start.8 = (bf16[1,4,2,32,1024]{4,3,2,1,0:T(8,128)(2,1)}, bf16[1,4,2,32,1024]{4,3,2,1,0:T(8,128)(2,1)}, u32[]{:S(2)}, u32[]{:S(2)}) collective-permute-start(bf16[1,4,2,32,1024]{4,3,2,1,0:T(8,128)(2,1)} %get-tuple-element.9), channel_id=1, source_target_pairs={{448,0},{456,8},{464,16},{472,24},{480,32},{488,40},{496,48},{504,... | collective-permute-start | bytes 1572872 | tf_op jit(solution)/shard_map/ppermute | solution.py:16
  157.9 25.8 %all-to-all-start.1 = ((bf16[8,48,2048]{2,1,0:T(8,128)(2,1)}), bf16[8,48,2048]{2,1,0:T(8,128)(2,1)}, u32[]{:S(2)}, u32[]{:S(2)}) async-start(bf16[8,48,2048]{2,1,0:T(8,128)(2,1)} %broadcast_in_dim.37), calls=%async_computation.1 | async-start | bytes 3145728 | tf_op jit(solution)/shard_map/all_to_all | solution.py:82
  177.0 12.8 %collective-permute-start.9 = (bf16[1024,1024]{1,0:T(8,128)(2,1)}, bf16[1024,1024]{1,0:T(8,128)(2,1)}, u32[]{:S(2)}, u32[]{:S(2)}) collective-permute-start(bf16[1024,1024]{1,0:T(8,128)(2,1)} %bitcast.137), channel_id=1, source_target_pairs={{0,1},{1,0},{2,3},{3,2},{4,5},{5,4},{6,7},{7,6},{8,9},{9,8},{10,11... | collective-permute-start | bytes 6291464 | tf_op jit(solution)/shard_map/ppermute | solution.py:69
  186.5 2.3 %copy-start.2 = (bf16[4,4,2,32,1024]{4,3,2,1,0:T(8,128)(2,1)S(1)}, bf16[4,4,2,32,1024]{4,3,2,1,0:T(8,128)(2,1)}, u32[]{:S(2)}) copy-start(bf16[4,4,2,32,1024]{4,3,2,1,0:T(8,128)(2,1)} %bitcast_dynamic-update-slice_fusion) | copy-start | bytes 6291460
  218.2 0.7 copy-start.7
